TPU v7x, 1024 devices: a whole 4x4x32 slice. The times are simulated.
1024 devices in a mesh: ep: 64 (over z, core), tp: 16 (over y, x).
Axes of the slice: x: 4, y: 4, z: 32, core: 2. Of those that a mesh axis runs over, the one named last changes fastest.
Arguments:
- tokens: bfloat16 [8192, 2048], P('ep', 'tp')
- norm_gain: float32 [2048], P('tp'), may hold values from 0.1 to 1.9
- routing: int32 [8192, 2], P('ep'), may hold values from 0 to 31, all different within a row; in each aligned block of 128 rows (0 to 127, 128 to 255, ...) at most 10 rows name the same one
- route_weight: float32 [8192, 2], P('ep'), may hold values from 0.1 to 1
- gate_weight: bfloat16 [64, 2048, 3584], P('ep', None, 'tp'), may hold values from -0.125 to 0.125
- up_weight: bfloat16 [64, 2048, 3584], P('ep', None, 'tp'), may hold values from -0.125 to 0.125
- down_weight: bfloat16 [64, 3584, 2048], P('ep', None, 'tp')
- final_gain: float32 [2048], P('tp'), may hold values from 0.1 to 1.9
Outputs:
- mixed: bfloat16 [8192, 2048], P('ep', 'tp')
Inputs may be any that keep to these rules, and one draw needn't show every extreme that they name: `routing`: each row names 2 different experts. Among the 128 rows of one device along ep (aligned blocks), no expert is named more than 10 times, a bound that some blocks reach.
All inputs are finite; a program needn't handle non-finite values.
Results may differ from a plain program's by a relative error of at most 0.0077.
Values may be sent and summed in bfloat16 or wider, within the bound.
No kernel may reach another device: no remote copies, remote signals or barrier semaphores. Data moves between devices by JAX's collectives and lax.ppermute only.
A program may use at most 32 MiB of HBM per device.

v0:
```python
import jax
import jax.numpy as jnp
from jax import lax
from jax.sharding import PartitionSpec as P

D = 2048
TOPK = 2


EPS = 1e-05


def sent_to_all(shard, axis):
    peers = lax.axis_size(axis)
    return lax.all_to_all(
        jnp.broadcast_to(shard[None], (peers, *shard.shape)), axis, 0, 0, tiled=True
    )


def taken_together(shard, axis):
    everything = sent_to_all(shard, axis)
    return jnp.sum(everything, axis=0)


def from_partner(shard, axis, apart):
    return lax.ppermute(shard, axis, [(i, i ^ 1 << apart) for i in range(lax.axis_size(axis))])


def joined_along(blocks, dim):
    blocks = jnp.moveaxis(blocks, 0, dim)
    dims = blocks.shape
    return blocks.reshape(*dims[:dim], dims[dim] * dims[dim + 1], *dims[dim + 2 :])


def collect(shard, axis, dim):
    blocks = sent_to_all(shard, axis)
    return joined_along(blocks, dim)


def shards(
    tokens, norm_gain, routing, route_weight, gate_weight, up_weight, down_weight, final_gain
):
    ep_count = lax.axis_size("ep")
    experts = ep_count // 2
    tok_rows = tokens.shape[0]
    width_local = tokens.shape[1]
    capacity = 2 * ((tok_rows * TOPK * 5 + experts * 8 - 1) // (experts * 8))
    half_cap = capacity // 2
    row_count = ep_count * capacity
    is_even = lax.axis_index("ep") % 2 == 0
    values_f = tokens.astype(jnp.float32)
    square_sum = taken_together(jnp.sum(values_f * values_f, axis=1), "tp")
    normed = (values_f * lax.rsqrt(square_sum / D + EPS)[:, None] * norm_gain).astype(jnp.bfloat16)
    expert_ids = routing.reshape(-1)
    onehot = (expert_ids[:, None] == jnp.arange(experts, dtype=jnp.int32)).astype(jnp.int32)
    slot_index = jnp.sum((jnp.cumsum(onehot, axis=0) - onehot) * onehot, axis=1)
    place_index = expert_ids * capacity + slot_index
    hit_table = (place_index[:, None] == jnp.arange(experts * capacity, dtype=jnp.int32)).astype(
        jnp.float32
    )
    hit_table = hit_table.reshape(tok_rows, TOPK, experts * capacity)
    picker = jnp.sum(hit_table, axis=1)
    weighted = jnp.sum(hit_table * route_weight[:, :, None], axis=1)
    contract = (((0,), (0,)), ((), ()))
    gate_local = gate_weight[0]
    up_local = up_weight[0]
    down_local = down_weight[0]
    outgoing = lax.dot_general(
        picker.astype(jnp.bfloat16), normed, contract, preferred_element_type=jnp.float32
    )
    outgoing = outgoing.astype(jnp.bfloat16).reshape(ep_count, half_cap, width_local)
    own_half = lax.all_to_all(outgoing, "ep", split_axis=0, concat_axis=0, tiled=True)
    partner_half = from_partner(own_half, "ep", 0)
    arrived = jnp.where(
        is_even,
        jnp.concatenate([own_half, partner_half], axis=1),
        jnp.concatenate([partner_half, own_half], axis=1),
    ).reshape(row_count, width_local)
    shard_piece = collect(arrived, "tp", 1)
    gate = jnp.dot(shard_piece, gate_local, preferred_element_type=jnp.float32)
    upper = jnp.dot(shard_piece, up_local, preferred_element_type=jnp.float32)
    hidden = (jax.nn.silu(gate) * upper).astype(jnp.bfloat16)
    half_out = jnp.dot(
        lax.all_gather(hidden, "tp", axis=1, tiled=True),
        down_local,
        preferred_element_type=jnp.float32,
    )
    half_out = half_out.astype(jnp.bfloat16).reshape(ep_count, capacity, width_local)
    partner_out = from_partner(half_out, "ep", 0)
    pair_sum = (half_out.astype(jnp.float32) + partner_out.astype(jnp.float32)).astype(jnp.bfloat16)
    start = jnp.where(is_even, 0, half_cap).astype(jnp.int32)
    own_slots = lax.dynamic_slice_in_dim(pair_sum, start, half_cap, 1)
    paired = lax.all_to_all(own_slots, "ep", split_axis=0, concat_axis=0, tiled=True)
    paired = lax.optimization_barrier(paired)
    paired = paired.reshape(experts * capacity, width_local).astype(jnp.float32)
    mixed_sum = jnp.dot(weighted, paired, precision=lax.Precision.HIGHEST)
    out_square = taken_together(jnp.sum(mixed_sum * mixed_sum, axis=1), "tp")
    return (mixed_sum * lax.rsqrt(out_square / D + EPS)[:, None] * final_gain).astype(jnp.bfloat16)


def solution(mesh):
    placed = (
        P("ep", "tp"),
        P("tp"),
        P("ep", None),
        P("ep", None),
        P("ep", None, "tp"),
        P("ep", None, "tp"),
        P("ep", None, "tp"),
        P("tp"),
    )
    return jax.shard_map(
        shards, mesh=mesh, in_specs=placed, out_specs=P("ep", "tp"), check_vma=False
    )
```

profile of v0, /device:TPU:32, one launch (start us, length us, event | category | flops | bytes accessed | tf_op | source)
XLA Modules:
  0.0 277.7 jit_solution(11340147714563079826)
XLA Ops:
  6.5 0.9 fusion.6
  7.5 0.6 broadcast_in_dim.6
  8.1 7.0 %all-to-all-start = ((f32[16,1,128]{2,1,0:T(1,128)}), f32[16,1,128]{2,1,0:T(1,128)S(1)}, u32[]{:S(2)}, u32[]{:S(2)}) async-start(f32[16,1,128]{2,1,0:T(1,128)} %broadcast_in_dim.6), calls=%async_computation | async-start | bytes 16384 | tf_op jit(solution)/shard_map/all_to_all | solution.py:15
  15.2 0.8 copy.38
  16.0 0.1 eq.48
  16.1 0.1 eq.44
  16.3 0.6 reduce-window.6
  16.9 0.2 slice_reduce_fusion
  17.1 0.1 fusion.12
  17.2 0.1 reduce_sum.66
  17.4 0.7 multiply_add_fusion
  18.1 0.8 convert_reduce_fusion
  18.9 3.8 %all-to-all-done = f32[16,1,128]{2,1,0:T(1,128)S(1)} async-done(((f32[16,1,128]{2,1,0:T(1,128)}), f32[16,1,128]{2,1,0:T(1,128)S(1)}, u32[]{:S(2)}, u32[]{:S(2)}) %all-to-all-start) | async-done | bytes 8224 | tf_op jit(solution)/shard_map/all_to_all | solution.py:15
  22.7 1.0 convolution_convert_fusion.1
  23.7 59.9 %all_to_all.27 = bf16[64,5,128]{2,1,0:T(8,128)(2,1)S(1)} all-to-all(bf16[64,5,128]{2,1,0:T(8,128)(2,1)S(1)} %reshape.84), channel_id=1, replica_groups=mesh['ep'=64,'tp'=16] {'ep'}, dimensions={0} | all-to-all | bytes 163840 | tf_op jit(solution)/shard_map/all_to_all | solution.py:72
  83.6 1.9 collective-permute-start
  85.5 1.3 collective-permute-done
  86.8 0.2 maximum_select_fusion
  87.1 0.2 copy.43
  87.2 0.3 broadcast_in_dim.7
  87.5 37.6 %all_to_all.28 = bf16[16,640,128]{1,2,0:T(8,128)(2,1)S(1)} all-to-all(bf16[16,640,128]{1,2,0:T(8,128)(2,1)S(1)} %broadcast_in_dim.7), channel_id=1, replica_groups=mesh['ep'=64,'tp'=16] {'tp'}, dimensions={0} | all-to-all | bytes 5242880 | tf_op jit(solution)/shard_map/all_to_all | solution.py:15
  125.1 0.9 fusion.3
  126.0 0.3 copy-done.2
  126.3 1.6 fusion
  127.9 67.3 %all-gather.2.cloned.1.call-done = bf16[640,3584]{0,1:T(8,128)(2,1)} async-done(((bf16[640,224]{0,1:T(8,128)(2,1)}), bf16[640,3584]{0,1:T(8,128)(2,1)}) %all-gather.2.cloned.1.call-update) | async-done | bytes 4587536 | tf_op jit(solution)/shard_map/all_gather | solution.py:84
  195.3 3.7 %convolution_convert_fusion = bf16[640,128]{1,0:T(8,128)(2,1)S(1)} fusion(bf16[640,3584]{0,1:T(8,128)(2,1)} %all-gather.2.cloned.1.call-done, bf16[1,3584,128]{2,1,0:T(8,128)(2,1)S(1)} %copy-done.3), kind=kOutput, calls=%fused_computation.2 | convolution fusion | flops 587284480 | bytes 5668864 | tf_op jit(solution)/shard_map/dot_general | solution.py:83
  199.0 1.9 collective-permute-start.1
  201.0 1.5 collective-permute-done.1
  202.6 54.4 %all_to_all.29 = bf16[64,5,128]{2,1,0:T(8,128)(2,1)S(1)} all-to-all(bf16[64,5,128]{2,1,0:T(8,128)(2,1)S(1)} %add_convert_fusion), channel_id=1, replica_groups=mesh['ep'=64,'tp'=16] {'ep'}, dimensions={0} | all-to-all | bytes 163840 | tf_op jit(solution)/shard_map/all_to_all | solution.py:93
  257.0 0.3 multiply_reduce_fusion
  257.4 12.6 %all_to_all.30 = f32[16,1,128]{2,1,0:T(1,128)S(1)} all-to-all(f32[16,1,128]{2,1,0:T(1,128)S(1)} %broadcast_in_dim.8), channel_id=1, replica_groups=mesh['ep'=64,'tp'=16] {'tp'}, dimensions={0} | all-to-all | bytes 16384 | tf_op jit(solution)/shard_map/all_to_all | solution.py:15
  270.1 0.7 copy.45
  (24 shorter events, 0.6 us)
Async XLA Ops:
  6.5 118.6 %copy-start = (bf16[1,2048,224]{1,2,0:T(8,128)(2,1)S(1)}, bf16[1,2048,224]{1,2,0:T(8,128)(2,1)}, u32[]{:S(2)}) copy-start(bf16[1,2048,224]{1,2,0:T(8,128)(2,1)} %param.12) | copy-start | bytes 2752516
  8.1 14.6 %all-to-all-start = ((f32[16,1,128]{2,1,0:T(1,128)}), f32[16,1,128]{2,1,0:T(1,128)S(1)}, u32[]{:S(2)}, u32[]{:S(2)}) async-start(f32[16,1,128]{2,1,0:T(1,128)} %broadcast_in_dim.6), calls=%async_computation | async-start | bytes 16384 | tf_op jit(solution)/shard_map/all_to_all | solution.py:15
  15.1 180.1 %all-gather.2.cloned.1.call-start = ((), (), s32[]{:S(2)}) async-start(), calls=%async_computation.5 | async-start | bytes 4874240 | tf_op jit(solution)/shard_map/all_gather | solution.py:84
  83.6 3.2 %collective-permute-start = (bf16[64,5,128]{2,1,0:T(8,128)(2,1)S(1)}, bf16[64,5,128]{2,1,0:T(8,128)(2,1)S(1)}, u32[]{:S(2)}, u32[]{:S(2)}) collective-permute-start(bf16[64,5,128]{2,1,0:T(8,128)(2,1)S(1)} %all_to_all.27), channel_id=1, source_target_pairs={{0,16},{16,0},{32,48},{48,32},{64,80},{80,64},{96,112},{112,96},{1... | collective-permute-start | bytes 245768 | tf_op jit(solution)/shard_map/ppermute | solution.py:26
  125.1 1.2 copy-start.2
  126.3 69.0 %copy-start.3 = (bf16[1,3584,128]{2,1,0:T(8,128)(2,1)S(1)}, bf16[1,3584,128]{2,1,0:T(8,128)(2,1)}, u32[]{:S(2)}) copy-start(bf16[1,3584,128]{2,1,0:T(8,128)(2,1)} %param.14) | copy-start | bytes 2752516
  127.9 142.1 %copy-start.1 = (f32[128]{0:T(128)S(1)}, f32[128]{0:T(128)}, u32[]{:S(2)}) copy-start(f32[128]{0:T(128)} %param.15) | copy-start | bytes 1540
  199.0 3.4 %collective-permute-start.1 = (bf16[64,10,128]{2,1,0:T(8,128)(2,1)S(1)}, bf16[64,10,128]{2,1,0:T(8,128)(2,1)S(1)}, u32[]{:S(2)}, u32[]{:S(2)}) collective-permute-start(bf16[64,10,128]{2,1,0:T(8,128)(2,1)S(1)} %reshape.86), channel_id=1, source_target_pairs={{0,16},{16,0},{32,48},{48,32},{64,80},{80,64},{96,112},{112,96},{1... | collective-permute-start | bytes 491528 | tf_op jit(solution)/shard_map/ppermute | solution.py:26
Sparse Core Ops, SparseCore 0:
  128.0 67.1 all-gather.1
where the time goes:
time: 278 us
  blocking collectives  164 us (59%)
  waiting for transfers between devices  73.9 us (27%)
  between operations  13.6 us (5%)
  starting transfers between devices  10.9 us (4%)
  matrix products  7.52 us (3%)
  local copies, waits for them, and re-layouts  3.78 us (1%)
  other arithmetic  3.54 us (1%)
    all_gather x1, waiting for transfers between devices, shards(): lax.all_gather(hidden, 'tp', axis=1, tiled=True)  67.3 us
    all_to_all x1, blocking collectives, shards(): lax.all_to_all(outgoing, 'ep', split_axis=0, concat_axis=0, tiled=True)  59.9 us
    all_to_all x1, blocking collectives, shards(): lax.all_to_all(own_slots, 'ep', split_axis=0, concat_axis=0, tiled=True)  54.4 us
    all_to_all x2, blocking collectives, sent_to_all(): lax.all_to_all(jnp.broadcast_to(shard[None], (peers, *shard.shape)), axis...  50.2 us
    all_to_all x1, starting transfers between devices, sent_to_all(): lax.all_to_all(jnp.broadcast_to(shard[None], (peers, *shard.shape)), axis...  7.03 us
  transfers between devices with their start and end apart: 4, of which 4 were waited for; matrix products, arithmetic and copies ran while one was open for 1% of the time, Pallas kernels for 0%

commit v1 on v0

v1 whole, which is shorter than its diff:
```python
import jax
import jax.numpy as jnp
from jax import lax
from jax.experimental import pallas as pl
from jax.experimental.pallas import tpu as pltpu
from jax.sharding import Mesh, PartitionSpec as P

D = 2048
EXPERTS = 32
TOK = 128
CAP = 10
ROWS = EXPERTS * CAP
TP = 16
W = D // TP
HID = 224
EXTRA = 8
EPS = 1e-05

VMEM = pl.BlockSpec(memory_space=pltpu.VMEM)
F32 = jnp.float32
BF16 = jnp.bfloat16


def call(kernel, out_shape, count, **kw):
    many = isinstance(out_shape, (tuple, list))
    return pl.pallas_call(
        kernel,
        out_shape=out_shape,
        in_specs=[VMEM] * count,
        out_specs=tuple(VMEM for _ in out_shape) if many else VMEM,
        **kw,
    )


def place_of(slot, expert):
    return (slot // 2) * (2 * EXPERTS) + 2 * expert + slot % 2


def dispatch_kernel(routing_ref, tokens_ref, gain_ref, out_ref, place_ref, gain_out_ref):
    routing = routing_ref[...]
    expert0, expert1 = routing[:, 0:1], routing[:, 1:2]
    lanes = lax.broadcasted_iota(jnp.int32, (TOK, 128), 1)
    hit0, hit1 = lanes == expert0, lanes == expert1
    both = jnp.where(hit0 | hit1, 1.0, 0.0).astype(BF16)
    earlier = jnp.where(
        lax.broadcasted_iota(jnp.int32, (TOK, TOK), 1)
        < lax.broadcasted_iota(jnp.int32, (TOK, TOK), 0),
        1.0,
        0.0,
    ).astype(BF16)
    before = jnp.dot(earlier, both, preferred_element_type=F32)
    slot0 = jnp.sum(jnp.where(hit0, before, 0.0), axis=1, keepdims=True).astype(jnp.int32)
    slot1 = jnp.sum(jnp.where(hit1, before, 0.0), axis=1, keepdims=True).astype(jnp.int32)
    place0, place1 = place_of(slot0, expert0), place_of(slot1, expert1)
    place_ref[...] = jnp.concatenate([place0, place1], axis=1)
    spots = lax.broadcasted_iota(jnp.int32, (TOK, ROWS), 1)
    picker = jnp.where((spots == place0) | (spots == place1), 1.0, 0.0).astype(BF16)
    rows = lax.dot_general(
        picker, tokens_ref[...], (((0,), (0,)), ((), ())), preferred_element_type=F32
    ).astype(BF16)
    for block in range(CAP // 2):
        out_ref[:, block * W : (block + 1) * W] = rows[block * 64 : (block + 1) * 64]
    gain = gain_ref[...]
    high = gain.astype(BF16).astype(F32)
    mid = (gain - high).astype(BF16).astype(F32)
    low = gain - high - mid
    index = lax.broadcasted_iota(jnp.int32, (EXTRA, W), 0)
    parts = jnp.where(index == 0, high, jnp.where(index == 1, mid, jnp.where(index == 2, low, 0.0)))
    gain_out_ref[...] = parts.astype(BF16)


def spread_kernel(rows_ref, gain_ref, out_ref):
    gain = gain_ref[...]
    for block in range(CAP // 2):
        piece = rows_ref[:, block * W : (block + 1) * W]
        for peer in range(TP):
            out_ref[peer, block * 64 : (block + 1) * 64] = piece
    for peer in range(TP):
        out_ref[peer, ROWS : ROWS + EXTRA] = gain


def experts_kernel(x_ref, gate_a, gate_b, up_a, up_b, down_a, down_b, out_ref, normed_ref):
    total = jnp.zeros((ROWS, W), F32)
    for t in range(TP):
        piece = x_ref[t, :ROWS].astype(F32)
        total = total + piece * piece
    scale = lax.rsqrt(jnp.sum(total, axis=1, keepdims=True) / D + EPS)
    for t in range(TP):
        gain = jnp.sum(x_ref[t, ROWS : ROWS + EXTRA].astype(F32), axis=0, keepdims=True)
        piece = x_ref[t, :ROWS].astype(F32)
        normed_ref[:, t * W : (t + 1) * W] = (piece * scale * gain).astype(BF16)
    normed = normed_ref[...]
    hidden = []
    for gate_ref, up_ref in ((gate_a, up_a), (gate_b, up_b)):
        gate = jnp.dot(normed, gate_ref[...], preferred_element_type=F32)
        upper = jnp.dot(normed, up_ref[...], preferred_element_type=F32)
        hidden.append((jax.nn.silu(gate) * upper).astype(BF16))
    for t in range(TP):
        part = jnp.dot(hidden[0], down_a[t], preferred_element_type=F32)
        part = part + jnp.dot(hidden[1], down_b[t], preferred_element_type=F32)
        out_ref[t] = part.astype(BF16)


def reduce_kernel(parts_ref, out_ref):
    for block in range(CAP // 2):
        total = jnp.zeros((64, W), F32)
        for t in range(TP):
            total = total + parts_ref[t, block * 64 : (block + 1) * 64].astype(F32)
        out_ref[:, block * W : (block + 1) * W] = total.astype(BF16)


def combine_kernel(rows_ref, place_ref, weight_ref, mixed_ref, square_ref):
    rows = jnp.concatenate(
        [rows_ref[:, block * W : (block + 1) * W] for block in range(CAP // 2)], axis=0
    )
    spots = lax.broadcasted_iota(jnp.int32, (TOK, ROWS), 1)
    mixed = jnp.zeros((TOK, W), F32)
    for k in range(2):
        pick = jnp.where(spots == place_ref[:, k : k + 1], 1.0, 0.0).astype(BF16)
        row = jnp.dot(pick, rows, preferred_element_type=F32)
        mixed = mixed + row * weight_ref[:, k : k + 1]
    mixed_ref[...] = mixed
    square = jnp.sum((mixed * mixed).T, axis=0, keepdims=True)
    for t in range(TP):
        square_ref[t] = square


def finish_kernel(mixed_ref, square_ref, gain_ref, out_ref):
    square = jnp.zeros((1, TOK), F32)
    for t in range(TP):
        square = square + square_ref[t]
    column = jnp.broadcast_to(lax.rsqrt(square / D + EPS), (TOK, TOK)).T
    out_ref[...] = (mixed_ref[...] * column * gain_ref[...]).astype(BF16)


def shards(
    tokens, norm_gain, routing, route_weight, gate_weight, up_weight, down_weight, final_gain
):
    swap = [(0, 1), (1, 0)]
    gate_own, up_own = gate_weight[0], up_weight[0]
    outgoing, place, gain_parts = call(
        dispatch_kernel,
        (
            jax.ShapeDtypeStruct((64, 640), BF16),
            jax.ShapeDtypeStruct((TOK, 2), jnp.int32),
            jax.ShapeDtypeStruct((EXTRA, W), BF16),
        ),
        3,
    )(routing, tokens, norm_gain.reshape(1, W))
    arrived = lax.all_to_all(
        outgoing.reshape(EXPERTS, 2, 640), "z", 0, 0, tiled=True
    ).reshape(64, 640)
    down_own = lax.all_to_all(
        down_weight.reshape(TP, HID, W), "t", 0, 0, tiled=True
    )
    gate_other = lax.ppermute(gate_own, "c", swap)
    up_other = lax.ppermute(up_own, "c", swap)
    down_other = lax.ppermute(down_own, "c", swap)
    spread = call(
        spread_kernel, jax.ShapeDtypeStruct((TP, ROWS + EXTRA, W), BF16), 2
    )(arrived, gain_parts)
    features = lax.all_to_all(spread, "t", 0, 0, tiled=True)
    parts = call(
        experts_kernel,
        jax.ShapeDtypeStruct((TP, ROWS, W), BF16),
        7,
        scratch_shapes=[pltpu.VMEM((ROWS, D), BF16)],
    )(features, gate_own, gate_other, up_own, up_other, down_own, down_other)
    parts = lax.all_to_all(parts, "t", 0, 0, tiled=True)
    reduced = call(reduce_kernel, jax.ShapeDtypeStruct((64, 640), BF16), 1)(parts)
    returned = lax.all_to_all(
        reduced.reshape(EXPERTS, 2, 640), "z", 0, 0, tiled=True
    ).reshape(64, 640)
    mixed, square = call(
        combine_kernel,
        (
            jax.ShapeDtypeStruct((TOK, W), F32),
            jax.ShapeDtypeStruct((TP, 1, TOK), F32),
        ),
        3,
    )(returned, place, route_weight)
    squares = lax.all_to_all(square, "t", 0, 0, tiled=True)
    return call(finish_kernel, jax.ShapeDtypeStruct((TOK, W), BF16), 3)(
        mixed, squares, final_gain.reshape(1, W)
    )


def solution(mesh):
    split = Mesh(mesh.devices.reshape(EXPERTS, 2, TP), ("z", "c", "t"))
    ep = ("z", "c")
    placed = (
        P(ep, "t"),
        P("t"),
        P(ep, None),
        P(ep, None),
        P(ep, None, "t"),
        P(ep, None, "t"),
        P(ep, None, "t"),
        P("t"),
    )
    return jax.shard_map(
        shards, mesh=split, in_specs=placed, out_specs=P(ep, "t"), check_vma=False
    )
```

time: 278 us -> 187 us (0.67)
  the two profiles are of different devices: /device:TPU:32 before, /device:TPU:2 now
where the time goes in v1:
time: 187 us; the launch traced here: 186 us
  blocking collectives  93.2 us (50%)
  waiting for transfers between devices  36.9 us (20%)
  starting transfers between devices  22.7 us (12%)
  Pallas kernels  17.4 us (9%)
  local copies, waits for them, and re-layouts  16 us (9%)
    all_to_all x1, blocking collectives, shards(): lax.all_to_all(outgoing.reshape(EXPERTS, 2, 640), 'z', 0, 0, tiled=True)  55.8 us
    all_to_all x1, waiting for transfers between devices, shards(): lax.all_to_all(reduced.reshape(EXPERTS, 2, 640), 'z', 0, 0, tiled=True)  25.7 us
    all_to_all x1, blocking collectives, shards(): parts = lax.all_to_all(parts, 't', 0, 0, tiled=True)  25.7 us
    all_to_all x1, blocking collectives, shards(): squares = lax.all_to_all(square, 't', 0, 0, tiled=True)  11.7 us
    all_to_all x1, waiting for transfers between devices, shards(): lax.all_to_all(down_weight.reshape(TP, HID, W), 't', 0, 0, tiled=True)  9.78 us
    unnamed x12, local copies, waits for them, and re-layouts  7.75 us
    all_to_all x1, starting transfers between devices, shards(): lax.all_to_all(down_weight.reshape(TP, HID, W), 't', 0, 0, tiled=True)  7.48 us
    pallas_call x1, Pallas kernels, shards(): call(experts_kernel, jax.ShapeDtypeStruct((TP, ROWS, W), BF16), 7, scratc...  7.42 us
  transfers between devices with their start and end apart: 6, of which 3 were waited for; matrix products, arithmetic and copies ran while one was open for 6% of the time, Pallas kernels for 1%

profile of v1, /device:TPU:2, one launch (start us, length us, event | category | flops | bytes accessed | tf_op | source)
XLA Modules:
  0.0 186.3 jit_solution(3306370475559157232)
XLA Ops:
  0.0 1.4 copy.13.routing_ref
  1.4 2.2 %shard_map.82 = (bf16[64,640]{1,0:T(8,128)(2,1)}, s32[128,2]{1,0:T(8,128)}, bf16[8,128]{1,0:T(8,128)(2,1)}) custom-call(s32[128,2]{1,0:T(8,128)} %copy.13.routing_ref, bf16[128,128]{1,0:T(8,128)(2,1)} %tokens_ref.1, f32[1,128]{1,0:T(1,128)} %bitcast.10), custom_call_target="tpu_custom_call" | custom-call | tf_op jit(solution)/shard_map/pallas_call | solution.py:141
  3.6 0.9 reshape.22
  4.5 55.8 %all_to_all.30 = bf16[32,2,640]{2,1,0:T(2,128)(2,1)S(1)} all-to-all(bf16[32,2,640]{2,1,0:T(2,128)(2,1)S(1)} %reshape.22), channel_id=1, replica_groups=mesh['z'=32,'c'=2,'t'=16] {'z'}, dimensions={0} | all-to-all | bytes 163840 | tf_op jit(solution)/shard_map/all_to_all | solution.py:150
  60.3 7.5 %all-to-all-start.2 = ((bf16[16,224,128]{2,1,0:T(8,128)(2,1)}), bf16[16,224,128]{2,1,0:T(8,128)(2,1)S(1)}, u32[]{:S(2)}, u32[]{:S(2)}) async-start(bf16[16,224,128]{2,1,0:T(8,128)(2,1)} %bitcast.9), calls=%async_computation.2 | async-start | bytes 1835008 | tf_op jit(solution)/shard_map/all_to_all | solution.py:153
  67.8 0.7 reshape.23.rows_ref
  68.5 2.1 %shard_map.83 = bf16[16,328,128]{2,1,0:T(8,128)(2,1)} custom-call(bf16[64,640]{1,0:T(8,128)(2,1)} %reshape.23.rows_ref, bf16[8,128]{1,0:T(8,128)(2,1)} %get-tuple-element.11.gain_ref), custom_call_target="tpu_custom_call" | custom-call | tf_op jit(solution)/shard_map/pallas_call | solution.py:159
  70.6 9.8 %all-to-all-done.2.down_a = bf16[16,224,128]{2,1,0:T(8,128)(2,1)S(1)} async-done(((bf16[16,224,128]{2,1,0:T(8,128)(2,1)}), bf16[16,224,128]{2,1,0:T(8,128)(2,1)S(1)}, u32[]{:S(2)}, u32[]{:S(2)}) %all-to-all-start.2) | async-done | bytes 917536 | tf_op jit(solution)/shard_map/all_to_all | solution.py:153
  80.4 4.9 %all-to-all-start.1 = ((bf16[16,328,128]{2,1,0:T(8,128)(2,1)}), bf16[16,328,128]{2,1,0:T(8,128)(2,1)S(1)}, u32[]{:S(2)}, u32[]{:S(2)}) async-start(bf16[16,328,128]{2,1,0:T(8,128)(2,1)} %shard_map.83), calls=%async_computation.1 | async-start | bytes 2686976 | tf_op jit(solution)/shard_map/all_to_all | solution.py:162
  85.3 1.9 %collective-permute-start = (bf16[2048,224]{0,1:T(8,128)(2,1)}, bf16[2048,224]{0,1:T(8,128)(2,1)}, u32[]{:S(2)}, u32[]{:S(2)}) collective-permute-start(bf16[2048,224]{0,1:T(8,128)(2,1)} %bitcast.2), channel_id=1, source_target_pairs={{0,16},{16,0},{1,17},{17,1},{2,18},{18,2},{3,19},{19,3},{4,20},{20... | collective-permute-start | bytes 2752520 | tf_op jit(solution)/shard_map/ppermute | solution.py:156
  87.2 2.4 %collective-permute-start.1 = (bf16[2048,224]{0,1:T(8,128)(2,1)}, bf16[2048,224]{0,1:T(8,128)(2,1)}, u32[]{:S(2)}, u32[]{:S(2)}) collective-permute-start(bf16[2048,224]{0,1:T(8,128)(2,1)} %bitcast.4), channel_id=1, source_target_pairs={{0,16},{16,0},{1,17},{17,1},{2,18},{18,2},{3,19},{19,3},{4,20},{20... | collective-permute-start | bytes 2752520 | tf_op jit(solution)/shard_map/ppermute | solution.py:157
  89.6 1.9 %collective-permute-start.2 = (bf16[16,224,128]{2,1,0:T(8,128)(2,1)S(1)}, bf16[16,224,128]{2,1,0:T(8,128)(2,1)S(1)}, u32[]{:S(2)}, u32[]{:S(2)}) collective-permute-start(bf16[16,224,128]{2,1,0:T(8,128)(2,1)S(1)} %all-to-all-done.2.down_a), channel_id=1, source_target_pairs={{0,16},{16,0},{1,17},{17,1},{2,18},{18,2},{3,19},{19,3},{4,20},{20... | collective-permute-start | bytes 2752520 | tf_op jit(solution)/shard_map/ppermute | solution.py:158
  91.5 2.2 %copy.14 = bf16[1,2048,224]{2,1,0:T(8,128)(2,1)} copy(bf16[1,2048,224]{1,2,0:T(8,128)(2,1)} %param.12) | data formatting | bytes 1835008 | tf_op args[4]
  93.8 2.3 %copy.16 = bf16[1,2048,224]{2,1,0:T(8,128)(2,1)} copy(bf16[1,2048,224]{1,2,0:T(8,128)(2,1)} %param.13) | data formatting | bytes 1835008 | tf_op args[5]
  96.1 0.0 collective-permute-done
  96.1 2.2 %copy.18.gate_b = bf16[2048,224]{1,0:T(8,128)(2,1)} copy(bf16[2048,224]{0,1:T(8,128)(2,1)} %collective-permute-done) | data formatting | bytes 1835008 | tf_op jit(solution)/shard_map/ppermute | solution.py:156
  98.3 0.0 collective-permute-done.1
  98.3 2.3 %copy.19.up_b = bf16[2048,224]{1,0:T(8,128)(2,1)} copy(bf16[2048,224]{0,1:T(8,128)(2,1)} %collective-permute-done.1) | data formatting | bytes 1835008 | tf_op jit(solution)/shard_map/ppermute | solution.py:157
  100.6 0.0 collective-permute-done.2.down_b
  100.6 1.3 all-to-all-done.1.x_ref
  101.9 1.1 copy-done
  103.0 7.4 %shard_map.84 = bf16[16,320,128]{2,1,0:T(8,128)(2,1)} custom-call(bf16[16,328,128]{2,1,0:T(8,128)(2,1)} %copy-done, bf16[2048,224]{1,0:T(8,128)(2,1)} %bitcast.7, bf16[2048,224]{1,0:T(8,128)(2,1)} %copy.18.gate_b, bf16[2048,224]{1,0:T(8,128)(2,1)} %bitcast.8, bf16[2048,224]{1,0:T(8,128)(2,1)} %copy.19.up_b, bf16[16,224,128]{2,1,0:T(8,128)(2,1)} %copy-done.1, ...), custom_call_target="tpu_custom_call" | custom-call | tf_op jit(solution)/shard_map/pallas_call | solution.py:163
  110.4 25.7 %all_to_all.31.parts_ref = bf16[16,320,128]{2,1,0:T(8,128)(2,1)} all-to-all(bf16[16,320,128]{2,1,0:T(8,128)(2,1)} %shard_map.84), channel_id=1, replica_groups=mesh['z'=32,'c'=2,'t'=16] {'t'}, dimensions={0} | all-to-all | bytes 2621440 | tf_op jit(solution)/shard_map/all_to_all | solution.py:169
  136.1 2.1 %shard_map.85 = bf16[64,640]{1,0:T(8,128)(2,1)} custom-call(bf16[16,320,128]{2,1,0:T(8,128)(2,1)} %all_to_all.31.parts_ref), custom_call_target="tpu_custom_call" | custom-call | tf_op jit(solution)/shard_map/pallas_call | solution.py:170
  138.2 1.5 reshape.25
  139.8 4.1 %all-to-all-start.4 = ((bf16[32,2,640]{2,1,0:T(2,128)(2,1)}), bf16[32,2,640]{2,1,0:T(2,128)(2,1)S(1)}, u32[]{:S(2)}, u32[]{:S(2)}) async-start(bf16[32,2,640]{2,1,0:T(2,128)(2,1)} %reshape.25), calls=%async_computation.4 | async-start | bytes 163840 | tf_op jit(solution)/shard_map/all_to_all | solution.py:171
  143.9 0.7 copy.20.weight_ref
  144.7 25.7 %all-to-all-done.4 = bf16[32,2,640]{2,1,0:T(2,128)(2,1)S(1)} async-done(((bf16[32,2,640]{2,1,0:T(2,128)(2,1)}), bf16[32,2,640]{2,1,0:T(2,128)(2,1)S(1)}, u32[]{:S(2)}, u32[]{:S(2)}) %all-to-all-start.4) | async-done | bytes 81952 | tf_op jit(solution)/shard_map/all_to_all | solution.py:171
  170.4 0.7 reshape.26.rows_ref
  171.1 1.9 %shard_map.86 = (f32[128,128]{1,0:T(8,128)}, f32[16,1,128]{2,1,0:T(1,128)}) custom-call(bf16[64,640]{1,0:T(8,128)(2,1)} %reshape.26.rows_ref, s32[128,2]{1,0:T(8,128)} %get-tuple-element.12.place_ref, f32[128,2]{1,0:T(8,128)} %copy.20.weight_ref), custom_call_target="tpu_custom_call" | custom-call | tf_op jit(solution)/shard_map/pallas_call | solution.py:174
  172.9 11.7 %all_to_all.32.square_ref = f32[16,1,128]{2,1,0:T(1,128)} all-to-all(f32[16,1,128]{2,1,0:T(1,128)} %get-tuple-element.14), channel_id=1, replica_groups=mesh['z'=32,'c'=2,'t'=16] {'t'}, dimensions={0} | all-to-all | bytes 16384 | tf_op jit(solution)/shard_map/all_to_all | solution.py:182
  184.7 1.6 shard_map.87
  (7 shorter events, 0.0 us)
Async XLA Ops:
  60.3 20.1 %all-to-all-start.2 = ((bf16[16,224,128]{2,1,0:T(8,128)(2,1)}), bf16[16,224,128]{2,1,0:T(8,128)(2,1)S(1)}, u32[]{:S(2)}, u32[]{:S(2)}) async-start(bf16[16,224,128]{2,1,0:T(8,128)(2,1)} %bitcast.9), calls=%async_computation.2 | async-start | bytes 1835008 | tf_op jit(solution)/shard_map/all_to_all | solution.py:153
  80.4 9.2 %copy-start.1 = (bf16[16,224,128]{2,1,0:T(8,128)(2,1)}, bf16[16,224,128]{2,1,0:T(8,128)(2,1)S(1)}, u32[]{:S(2)}) copy-start(bf16[16,224,128]{2,1,0:T(8,128)(2,1)S(1)} %all-to-all-done.2.down_a) | copy-start | bytes 2752516
  80.4 21.5 %all-to-all-start.1 = ((bf16[16,328,128]{2,1,0:T(8,128)(2,1)}), bf16[16,328,128]{2,1,0:T(8,128)(2,1)S(1)}, u32[]{:S(2)}, u32[]{:S(2)}) async-start(bf16[16,328,128]{2,1,0:T(8,128)(2,1)} %shard_map.83), calls=%async_computation.1 | async-start | bytes 2686976 | tf_op jit(solution)/shard_map/all_to_all | solution.py:162
  85.3 10.8 %collective-permute-start = (bf16[2048,224]{0,1:T(8,128)(2,1)}, bf16[2048,224]{0,1:T(8,128)(2,1)}, u32[]{:S(2)}, u32[]{:S(2)}) collective-permute-start(bf16[2048,224]{0,1:T(8,128)(2,1)} %bitcast.2), channel_id=1, source_target_pairs={{0,16},{16,0},{1,17},{17,1},{2,18},{18,2},{3,19},{19,3},{4,20},{20... | collective-permute-start | bytes 2752520 | tf_op jit(solution)/shard_map/ppermute | solution.py:156
  87.2 11.1 %collective-permute-start.1 = (bf16[2048,224]{0,1:T(8,128)(2,1)}, bf16[2048,224]{0,1:T(8,128)(2,1)}, u32[]{:S(2)}, u32[]{:S(2)}) collective-permute-start(bf16[2048,224]{0,1:T(8,128)(2,1)} %bitcast.4), channel_id=1, source_target_pairs={{0,16},{16,0},{1,17},{17,1},{2,18},{18,2},{3,19},{19,3},{4,20},{20... | collective-permute-start | bytes 2752520 | tf_op jit(solution)/shard_map/ppermute | solution.py:157
  89.6 11.0 %collective-permute-start.2 = (bf16[16,224,128]{2,1,0:T(8,128)(2,1)S(1)}, bf16[16,224,128]{2,1,0:T(8,128)(2,1)S(1)}, u32[]{:S(2)}, u32[]{:S(2)}) collective-permute-start(bf16[16,224,128]{2,1,0:T(8,128)(2,1)S(1)} %all-to-all-done.2.down_a), channel_id=1, source_target_pairs={{0,16},{16,0},{1,17},{17,1},{2,18},{18,2},{3,19},{19,3},{4,20},{20... | collective-permute-start | bytes 2752520 | tf_op jit(solution)/shard_map/ppermute | solution.py:158
  100.6 1.3 copy-start.2
  101.9 1.1 copy-start
  136.1 7.8 %copy-start.3 = (f32[128,2]{0,1:T(2,128)S(1)}, f32[128,2]{0,1:T(2,128)}, u32[]{:S(2)}) copy-start(f32[128,2]{0,1:T(2,128)} %param.11) | copy-start | bytes 3076
  139.8 30.6 %all-to-all-start.4 = ((bf16[32,2,640]{2,1,0:T(2,128)(2,1)}), bf16[32,2,640]{2,1,0:T(2,128)(2,1)S(1)}, u32[]{:S(2)}, u32[]{:S(2)}) async-start(bf16[32,2,640]{2,1,0:T(2,128)(2,1)} %reshape.25), calls=%async_computation.4 | async-start | bytes 163840 | tf_op jit(solution)/shard_map/all_to_all | solution.py:171

commit v2 on v1

v2 whole, which is shorter than its diff:
```python
import jax
import jax.numpy as jnp
from jax import lax
from jax.experimental import pallas as pl
from jax.experimental.pallas import tpu as pltpu
from jax.sharding import Mesh, PartitionSpec as P


D = 2048
EXPERTS = 32
TOK = 128
CAP = 10
ROWS = EXPERTS * CAP
TP = 16
W = D // TP
HID = 224
EXTRA = 8
EPS = 1e-05

F32 = jnp.float32
BF16 = jnp.bfloat16
MIB = 1 << 20


def call(kernel, outs, mib, free=0, **kw):
    def run(*operands):
        near = operands[: len(operands) - free]
        far = operands[len(operands) - free :]
        many = isinstance(outs, list)
        vmem = pl.BlockSpec(memory_space=pltpu.VMEM)
        return pl.pallas_call(
            kernel,
            out_shape=[pltpu.VMEM(s, d) for s, d in outs] if many else pltpu.VMEM(*outs),
            in_specs=[vmem] * len(near) + [pl.BlockSpec(memory_space=pl.ANY)] * free,
            out_specs=[vmem] * len(outs) if many else vmem,
            compiler_params=pltpu.CompilerParams(vmem_limit_bytes=mib * MIB),
            **kw,
        )(*[pltpu.with_memory_space_constraint(x, pltpu.VMEM) for x in near], *far)

    return run


def place_of(slot, expert):
    return (slot // 2) * (2 * EXPERTS) + 2 * expert + slot % 2


def dispatch_kernel(routing_ref, tokens_ref, gain_ref, out_ref, place_ref, gain_out_ref):
    expert0, expert1 = routing_ref[0:1], routing_ref[1:2]
    index = lax.broadcasted_iota(jnp.int32, (EXPERTS, TOK), 0)
    hit0, hit1 = index == expert0, index == expert1
    both = jnp.where(hit0 | hit1, 1.0, 0.0).astype(BF16)
    earlier = jnp.where(
        lax.broadcasted_iota(jnp.int32, (TOK, TOK), 0)
        < lax.broadcasted_iota(jnp.int32, (TOK, TOK), 1),
        1.0,
        0.0,
    ).astype(BF16)
    before = jnp.dot(both, earlier, preferred_element_type=F32)
    slot0 = jnp.sum(jnp.where(hit0, before, 0.0), axis=0, keepdims=True).astype(jnp.int32)
    slot1 = jnp.sum(jnp.where(hit1, before, 0.0), axis=0, keepdims=True).astype(jnp.int32)
    place0, place1 = place_of(slot0, expert0), place_of(slot1, expert1)
    place_ref[0:1] = place0
    place_ref[1:2] = place1
    spots = lax.broadcasted_iota(jnp.int32, (ROWS, TOK), 0)
    picker = jnp.where((spots == place0) | (spots == place1), 1.0, 0.0).astype(BF16)
    rows = jnp.dot(picker, tokens_ref[...], preferred_element_type=F32).astype(BF16)
    for block in range(CAP // 2):
        piece = rows[block * 64 : (block + 1) * 64]
        out_ref[:, :, block * W : (block + 1) * W] = piece.reshape(EXPERTS, 2, W)
    gain = gain_ref[...]
    high = gain.astype(BF16).astype(F32)
    mid = (gain - high).astype(BF16).astype(F32)
    low = gain - high - mid
    part = lax.broadcasted_iota(jnp.int32, (EXTRA, W), 0)
    parts = jnp.where(part == 0, high, jnp.where(part == 1, mid, jnp.where(part == 2, low, 0.0)))
    gain_out_ref[...] = parts.astype(BF16)


def prepare_kernel(place_ref, weight_ref, pick_ref, weight_out_ref):
    spots = lax.broadcasted_iota(jnp.int32, (TOK, ROWS), 1).astype(F32)
    for k in range(2):
        place = jnp.broadcast_to(place_ref[k : k + 1].astype(F32), (TOK, TOK)).T
        pick_ref[k] = jnp.where(spots == place[:, 0:1], 1.0, 0.0).astype(BF16)
        weight_out_ref[k] = jnp.broadcast_to(weight_ref[k : k + 1], (TOK, TOK)).T


def spread_kernel(rows_ref, gain_ref, out_ref):
    gain = gain_ref[...]
    for block in range(CAP // 2):
        piece = rows_ref[:, :, block * W : (block + 1) * W].reshape(64, W)
        for peer in range(TP):
            out_ref[peer, block * 64 : (block + 1) * 64] = piece
    for peer in range(TP):
        out_ref[peer, ROWS : ROWS + EXTRA] = gain


def experts_kernel(x_ref, gate_a, gate_b, up_a, up_b, down_a, down_b, out_ref, normed_ref):
    total = jnp.zeros((ROWS, W), F32)
    for t in range(TP):
        piece = x_ref[t, :ROWS].astype(F32)
        total = total + piece * piece
    scale = lax.rsqrt(jnp.sum(total, axis=1, keepdims=True) / D + EPS)
    for t in range(TP):
        gain = jnp.sum(x_ref[t, ROWS : ROWS + EXTRA].astype(F32), axis=0, keepdims=True)
        piece = x_ref[t, :ROWS].astype(F32)
        normed_ref[:, t * W : (t + 1) * W] = (piece * scale * gain).astype(BF16)
    normed = normed_ref[...]
    hidden = []
    across = (((1,), (1,)), ((), ()))
    for gate_ref, up_ref in ((gate_a, up_a), (gate_b, up_b)):
        gate = lax.dot_general(normed, gate_ref[...], across, preferred_element_type=F32)
        upper = lax.dot_general(normed, up_ref[...], across, preferred_element_type=F32)
        hidden.append((jax.nn.silu(gate) * upper).astype(BF16))
    for t in range(TP):
        part = jnp.dot(hidden[0], down_a[t], preferred_element_type=F32)
        part = part + jnp.dot(hidden[1], down_b[t], preferred_element_type=F32)
        out_ref[t] = part.astype(BF16)


def reduce_kernel(parts_ref, out_ref):
    for block in range(CAP // 2):
        total = jnp.zeros((64, W), F32)
        for t in range(TP):
            total = total + parts_ref[t, block * 64 : (block + 1) * 64].astype(F32)
        out_ref[:, :, block * W : (block + 1) * W] = total.astype(BF16).reshape(EXPERTS, 2, W)


def combine_kernel(rows_ref, pick_ref, weight_ref, mixed_ref, square_ref):
    rows = jnp.concatenate(
        [
            rows_ref[:, :, block * W : (block + 1) * W].reshape(64, W)
            for block in range(CAP // 2)
        ],
        axis=0,
    )
    mixed = jnp.zeros((TOK, W), F32)
    for k in range(2):
        row = jnp.dot(pick_ref[k], rows, preferred_element_type=F32)
        mixed = mixed + row * weight_ref[k]
    mixed_ref[...] = mixed
    square = jnp.sum((mixed * mixed).T, axis=0, keepdims=True)
    for t in range(TP):
        square_ref[t] = square


def finish_kernel(mixed_ref, square_ref, gain_ref, out_ref):
    square = jnp.zeros((1, TOK), F32)
    for t in range(TP):
        square = square + square_ref[t]
    column = jnp.broadcast_to(lax.rsqrt(square / D + EPS), (TOK, TOK)).T
    out_ref[...] = (mixed_ref[...] * column * gain_ref[...]).astype(BF16)


def shards(
    tokens, norm_gain, routing, route_weight, gate_weight, up_weight, down_weight, final_gain
):
    swap = [(0, 1), (1, 0)]
    gate_own, up_own = gate_weight[0].T, up_weight[0].T
    outgoing, place, gain_parts = call(
        dispatch_kernel,
        [((EXPERTS, 2, 640), BF16), ((2, TOK), jnp.int32), ((EXTRA, W), BF16)],
        4,
    )(routing.T, tokens, norm_gain.reshape(1, W))
    arrived = lax.all_to_all(outgoing, "z", 0, 0, tiled=True)
    down_own = lax.all_to_all(down_weight.reshape(TP, HID, W), "t", 0, 0, tiled=True)
    gate_other = lax.ppermute(gate_own, "c", swap)
    up_other = lax.ppermute(up_own, "c", swap)
    down_other = lax.ppermute(down_own, "c", swap)
    pick, weight = call(
        prepare_kernel,
        [((2, TOK, ROWS), BF16), ((2, TOK, W), F32)],
        4,
    )(place, route_weight.T)
    spread = call(spread_kernel, ((TP, ROWS + EXTRA, W), BF16), 4)(arrived, gain_parts)
    features = lax.all_to_all(spread, "t", 0, 0, tiled=True)
    parts = call(
        experts_kernel,
        ((TP, ROWS, W), BF16),
        24,
        scratch_shapes=[pltpu.VMEM((ROWS, D), BF16)],
    )(features, gate_own, gate_other, up_own, up_other, down_own, down_other)
    parts = lax.all_to_all(parts, "t", 0, 0, tiled=True)
    reduced = call(reduce_kernel, ((EXPERTS, 2, 640), BF16), 4)(parts)
    returned = lax.all_to_all(reduced, "z", 0, 0, tiled=True)
    mixed, square = call(
        combine_kernel, [((TOK, W), F32), ((TP, 1, TOK), F32)], 4
    )(returned, pick, weight)
    squares = lax.all_to_all(square, "t", 0, 0, tiled=True)
    return call(finish_kernel, ((TOK, W), BF16), 4)(mixed, squares, final_gain.reshape(1, W))


def solution(mesh):
    split = Mesh(mesh.devices.reshape(EXPERTS, 2, TP), ("z", "c", "t"))
    ep = ("z", "c")
    placed = (
        P(ep, "t"),
        P("t"),
        P(ep, None),
        P(ep, None),
        P(ep, None, "t"),
        P(ep, None, "t"),
        P(ep, None, "t"),
        P("t"),
    )
    return jax.shard_map(
        shards, mesh=split, in_specs=placed, out_specs=P(ep, "t"), check_vma=False
    )
```

time: 187 us -> 175 us (0.936)
  Pallas kernels: 17.4 us -> 6.52 us
  blocking collectives: 93.2 us -> 85.6 us
  waiting for transfers between devices: 36.9 us -> 44.1 us
  local copies, waits for them, and re-layouts: 16 us -> 10.2 us
  starting transfers between devices: 22.7 us -> 27.2 us
    pallas_call x6 -> x7, Pallas kernels: 17.4 us -> 6.52 us  [run(): pl.pallas_call(kernel, out_shape=[pltpu.VMEM(s, d) for s, d in outs] if m...]
    all_to_all x1, blocking collectives: 25.7 us -> 19.4 us  [shards(): parts = lax.all_to_all(parts, 't', 0, 0, tiled=True)]
    all_to_all x1, waiting for transfers between devices: 1.33 us -> 6.98 us  [shards(): features = lax.all_to_all(spread, 't', 0, 0, tiled=True)]
    ppermute x2 -> x0, local copies, waits for them, and re-layouts: 4.5 us -> none  [the longest x1 2.25 us: shards(): up_other = lax.ppermute(up_own, 'c', swap)]
    all_to_all x1, starting transfers between devices: 4.14 us -> 8.58 us  [shards(): returned = lax.all_to_all(reduced, 'z', 0, 0, tiled=True)]
    reshape x4 -> x0, local copies, waits for them, and re-layouts: 3.77 us -> none  [the longest x1 1.54 us: shards(): reduced.reshape(EXPERTS, 2, 640)]
    unnamed x12 -> x27, local copies, waits for them, and re-layouts: 7.75 us -> 10.2 us
  transfers between devices with their start and end apart: 6 -> 6, of which waited for: 3 -> 4; matrix products, arithmetic and copies ran while one was open for 6% -> 0% of each run, Pallas kernels for 1% -> 1%
where the time goes in v2:
time: 175 us; the launch traced here: 174 us
  blocking collectives  85.6 us (49%)
  waiting for transfers between devices  44.1 us (25%)
  starting transfers between devices  27.2 us (16%)
  local copies, waits for them, and re-layouts  10.2 us (6%)
  Pallas kernels  6.52 us (4%)
    all_to_all x1, blocking collectives, shards(): arrived = lax.all_to_all(outgoing, 'z', 0, 0, tiled=True)  55.8 us
    all_to_all x1, waiting for transfers between devices, shards(): returned = lax.all_to_all(reduced, 'z', 0, 0, tiled=True)  25.4 us
    all_to_all x1, blocking collectives, shards(): parts = lax.all_to_all(parts, 't', 0, 0, tiled=True)  19.4 us
    all_to_all x1, waiting for transfers between devices, shards(): lax.all_to_all(down_weight.reshape(TP, HID, W), 't', 0, 0, tiled=True)  11.1 us
    all_to_all x1, blocking collectives, shards(): squares = lax.all_to_all(square, 't', 0, 0, tiled=True)  10.5 us
    unnamed x27, local copies, waits for them, and re-layouts  10.2 us
    all_to_all x1, starting transfers between devices, shards(): returned = lax.all_to_all(reduced, 'z', 0, 0, tiled=True)  8.58 us
    all_to_all x1, starting transfers between devices, shards(): lax.all_to_all(down_weight.reshape(TP, HID, W), 't', 0, 0, tiled=True)  7.48 us
  transfers between devices with their start and end apart: 6, of which 4 were waited for; matrix products, arithmetic and copies ran while one was open for 0% of the time, Pallas kernels for 1%

profile of v2, /device:TPU:2, one launch (start us, length us, event | category | flops | bytes accessed | tf_op | source)
XLA Modules:
  0.0 173.8 jit_solution(8415905822270165108)
XLA Ops:
  0.0 0.8 copy-done.8
  0.8 0.7 copy-done.9
  1.4 0.7 copy-done.11
  2.1 0.3 shard_map.82
  2.4 55.8 %all_to_all.30.rows_ref = bf16[32,2,640]{2,1,0:T(2,128)(2,1)S(1)} all-to-all(bf16[32,2,640]{2,1,0:T(2,128)(2,1)S(1)} %get-tuple-element.12), channel_id=1, replica_groups=mesh['z'=32,'c'=2,'t'=16] {'z'}, dimensions={0} | all-to-all | bytes 163840 | tf_op jit(solution)/shard_map/all_to_all | solution.py:164
  58.2 7.5 %all-to-all-start.2 = ((bf16[16,224,128]{2,1,0:T(8,128)(2,1)}), bf16[16,224,128]{2,1,0:T(8,128)(2,1)S(1)}, u32[]{:S(2)}, u32[]{:S(2)}) async-start(bf16[16,224,128]{2,1,0:T(8,128)(2,1)} %bitcast.19), calls=%async_computation.2 | async-start | bytes 1835008 | tf_op jit(solution)/shard_map/all_to_all | solution.py:165
  65.7 1.4 shard_map.83
  67.2 11.1 %all-to-all-done.2.down_a = bf16[16,224,128]{2,1,0:T(8,128)(2,1)S(1)} async-done(((bf16[16,224,128]{2,1,0:T(8,128)(2,1)}), bf16[16,224,128]{2,1,0:T(8,128)(2,1)S(1)}, u32[]{:S(2)}, u32[]{:S(2)}) %all-to-all-start.2) | async-done | bytes 917536 | tf_op jit(solution)/shard_map/all_to_all | solution.py:165
  78.3 4.9 %all-to-all-start.1 = ((bf16[16,328,128]{2,1,0:T(8,128)(2,1)}), bf16[16,328,128]{2,1,0:T(8,128)(2,1)S(1)}, u32[]{:S(2)}, u32[]{:S(2)}) async-start(bf16[16,328,128]{2,1,0:T(8,128)(2,1)} %shard_map.83), calls=%async_computation.1 | async-start | bytes 2686976 | tf_op jit(solution)/shard_map/all_to_all | solution.py:175
  83.2 1.9 %collective-permute-start = (bf16[224,2048]{1,0:T(8,128)(2,1)S(1)}, bf16[224,2048]{1,0:T(8,128)(2,1)S(1)}, u32[]{:S(2)}, u32[]{:S(2)}) collective-permute-start(bf16[224,2048]{1,0:T(8,128)(2,1)S(1)} %bitcast.11), channel_id=1, source_target_pairs={{0,16},{16,0},{1,17},{17,1},{2,18},{18,2},{3,19},{19,3},{4,20},{20... | collective-permute-start | bytes 2752520 | tf_op jit(solution)/shard_map/ppermute | solution.py:166
  85.1 2.4 %collective-permute-start.1 = (bf16[224,2048]{1,0:T(8,128)(2,1)}, bf16[224,2048]{1,0:T(8,128)(2,1)S(1)}, u32[]{:S(2)}, u32[]{:S(2)}) collective-permute-start(bf16[224,2048]{1,0:T(8,128)(2,1)} %bitcast.13), channel_id=1, source_target_pairs={{0,16},{16,0},{1,17},{17,1},{2,18},{18,2},{3,19},{19,3},{4,20},{20... | collective-permute-start | bytes 2752520 | tf_op jit(solution)/shard_map/ppermute | solution.py:167
  87.5 1.9 %collective-permute-start.2 = (bf16[16,224,128]{2,1,0:T(8,128)(2,1)S(1)}, bf16[16,224,128]{2,1,0:T(8,128)(2,1)S(1)}, u32[]{:S(2)}, u32[]{:S(2)}) collective-permute-start(bf16[16,224,128]{2,1,0:T(8,128)(2,1)S(1)} %all-to-all-done.2.down_a), channel_id=1, source_target_pairs={{0,16},{16,0},{1,17},{17,1},{2,18},{18,2},{3,19},{19,3},{4,20},{20... | collective-permute-start | bytes 2752520 | tf_op jit(solution)/shard_map/ppermute | solution.py:168
  89.5 0.0 collective-permute-done.gate_b
  89.5 0.9 copy-done.2
  90.4 0.9 copy-done.4
  91.3 0.6 collective-permute-done.2.down_b
  91.9 0.9 copy-done.6
  92.8 7.0 %all-to-all-done.1.x_ref = bf16[16,328,128]{2,1,0:T(8,128)(2,1)S(1)} async-done(((bf16[16,328,128]{2,1,0:T(8,128)(2,1)}), bf16[16,328,128]{2,1,0:T(8,128)(2,1)S(1)}, u32[]{:S(2)}, u32[]{:S(2)}) %all-to-all-start.1) | async-done | bytes 1343520 | tf_op jit(solution)/shard_map/all_to_all | solution.py:175
  99.8 1.2 copy-done.1
  101.0 1.2 copy-done.3
  102.2 1.2 copy-done.5
  103.4 1.2 copy-done.7
  104.5 3.2 %shard_map.84 = bf16[16,320,128]{2,1,0:T(8,128)(2,1)S(1)} custom-call(bf16[16,328,128]{2,1,0:T(8,128)(2,1)S(1)} %all-to-all-done.1.x_ref, bf16[224,2048]{1,0:T(8,128)(2,1)S(1)} %bitcast.12, bf16[224,2048]{1,0:T(8,128)(2,1)S(1)} %copy-done.3, bf16[224,2048]{1,0:T(8,128)(2,1)S(1)} %bitcast.14, bf16[224,2048]{1,0:T(8,128)(2,1)S(1)} %copy-done.5, ...), custom_call_target="tpu_custom_call" | custom-call | tf_op jit(solution)/shard_map/pallas_call | solution.py:31
  107.8 19.4 %all_to_all.31.parts_ref = bf16[16,320,128]{2,1,0:T(8,128)(2,1)S(1)} all-to-all(bf16[16,320,128]{2,1,0:T(8,128)(2,1)S(1)} %shard_map.84), channel_id=1, replica_groups=mesh['z'=32,'c'=2,'t'=16] {'t'}, dimensions={0} | all-to-all | bytes 2621440 | tf_op jit(solution)/shard_map/all_to_all | solution.py:182
  127.2 0.8 shard_map.85
  128.0 8.6 %all-to-all-start.4 = ((bf16[32,2,640]{2,1,0:T(2,128)(2,1)}), bf16[32,2,640]{2,1,0:T(2,128)(2,1)S(1)}, u32[]{:S(2)}, u32[]{:S(2)}) async-start(bf16[32,2,640]{2,1,0:T(2,128)(2,1)} %shard_map.85), calls=%async_computation.4 | async-start | bytes 163840 | tf_op jit(solution)/shard_map/all_to_all | solution.py:184
  136.6 0.2 shard_map.86
  136.8 25.4 %all-to-all-done.4.rows_ref = bf16[32,2,640]{2,1,0:T(2,128)(2,1)S(1)} async-done(((bf16[32,2,640]{2,1,0:T(2,128)(2,1)}), bf16[32,2,640]{2,1,0:T(2,128)(2,1)S(1)}, u32[]{:S(2)}, u32[]{:S(2)}) %all-to-all-start.4) | async-done | bytes 81952 | tf_op jit(solution)/shard_map/all_to_all | solution.py:184
  162.3 0.3 shard_map.87
  162.6 10.5 %all_to_all.32.square_ref = f32[16,1,128]{2,1,0:T(1,128)S(1)} all-to-all(f32[16,1,128]{2,1,0:T(1,128)S(1)} %get-tuple-element.18), channel_id=1, replica_groups=mesh['z'=32,'c'=2,'t'=16] {'t'}, dimensions={0} | all-to-all | bytes 16384 | tf_op jit(solution)/shard_map/all_to_all | solution.py:188
  173.1 0.1 shard_map.88
  173.2 0.6 copy.9
  (17 shorter events, 0.0 us)
Async XLA Ops:
  0.0 0.8 copy-start.8
  0.8 0.7 copy-start.9
  1.4 0.7 copy-start.11
  58.2 20.1 %all-to-all-start.2 = ((bf16[16,224,128]{2,1,0:T(8,128)(2,1)}), bf16[16,224,128]{2,1,0:T(8,128)(2,1)S(1)}, u32[]{:S(2)}, u32[]{:S(2)}) async-start(bf16[16,224,128]{2,1,0:T(8,128)(2,1)} %bitcast.19), calls=%async_computation.2 | async-start | bytes 1835008 | tf_op jit(solution)/shard_map/all_to_all | solution.py:165
  67.2 16.0 %copy-start = (bf16[1,2048,224]{1,2,0:T(8,128)(2,1)S(1)}, bf16[1,2048,224]{1,2,0:T(8,128)(2,1)}, u32[]{:S(2)}) copy-start(bf16[1,2048,224]{1,2,0:T(8,128)(2,1)} %param.12) | copy-start | bytes 2752516
  78.3 21.5 %all-to-all-start.1 = ((bf16[16,328,128]{2,1,0:T(8,128)(2,1)}), bf16[16,328,128]{2,1,0:T(8,128)(2,1)S(1)}, u32[]{:S(2)}, u32[]{:S(2)}) async-start(bf16[16,328,128]{2,1,0:T(8,128)(2,1)} %shard_map.83), calls=%async_computation.1 | async-start | bytes 2686976 | tf_op jit(solution)/shard_map/all_to_all | solution.py:175
  83.2 6.3 %collective-permute-start = (bf16[224,2048]{1,0:T(8,128)(2,1)S(1)}, bf16[224,2048]{1,0:T(8,128)(2,1)S(1)}, u32[]{:S(2)}, u32[]{:S(2)}) collective-permute-start(bf16[224,2048]{1,0:T(8,128)(2,1)S(1)} %bitcast.11), channel_id=1, source_target_pairs={{0,16},{16,0},{1,17},{17,1},{2,18},{18,2},{3,19},{19,3},{4,20},{20... | collective-permute-start | bytes 2752520 | tf_op jit(solution)/shard_map/ppermute | solution.py:166
  85.1 5.3 %collective-permute-start.1 = (bf16[224,2048]{1,0:T(8,128)(2,1)}, bf16[224,2048]{1,0:T(8,128)(2,1)S(1)}, u32[]{:S(2)}, u32[]{:S(2)}) collective-permute-start(bf16[224,2048]{1,0:T(8,128)(2,1)} %bitcast.13), channel_id=1, source_target_pairs={{0,16},{16,0},{1,17},{17,1},{2,18},{18,2},{3,19},{19,3},{4,20},{20... | collective-permute-start | bytes 2752520 | tf_op jit(solution)/shard_map/ppermute | solution.py:167
  87.5 4.4 %collective-permute-start.2 = (bf16[16,224,128]{2,1,0:T(8,128)(2,1)S(1)}, bf16[16,224,128]{2,1,0:T(8,128)(2,1)S(1)}, u32[]{:S(2)}, u32[]{:S(2)}) collective-permute-start(bf16[16,224,128]{2,1,0:T(8,128)(2,1)S(1)} %all-to-all-done.2.down_a), channel_id=1, source_target_pairs={{0,16},{16,0},{1,17},{17,1},{2,18},{18,2},{3,19},{19,3},{4,20},{20... | collective-permute-start | bytes 2752520 | tf_op jit(solution)/shard_map/ppermute | solution.py:168
  89.5 0.9 copy-start.2
  90.4 0.9 copy-start.4
  91.9 0.9 copy-start.6
  99.8 1.2 copy-start.1
  101.0 1.2 copy-start.3
  102.2 1.2 copy-start.5
  103.4 1.2 copy-start.7
  127.2 9.4 %copy-start.10 = (f32[128,2]{0,1:T(2,128)S(1)}, f32[128,2]{0,1:T(2,128)}, u32[]{:S(2)}) copy-start(f32[128,2]{0,1:T(2,128)} %param.11) | copy-start | bytes 3076
  127.2 45.9 %copy-start.12 = (f32[128]{0:T(128)S(1)}, f32[128]{0:T(128)}, u32[]{:S(2)}) copy-start(f32[128]{0:T(128)} %param.15) | copy-start | bytes 1540
  128.0 34.3 %all-to-all-start.4 = ((bf16[32,2,640]{2,1,0:T(2,128)(2,1)}), bf16[32,2,640]{2,1,0:T(2,128)(2,1)S(1)}, u32[]{:S(2)}, u32[]{:S(2)}) async-start(bf16[32,2,640]{2,1,0:T(2,128)(2,1)} %shard_map.85), calls=%async_computation.4 | async-start | bytes 163840 | tf_op jit(solution)/shard_map/all_to_all | solution.py:184

commit v3 on v2

--- a/solution.py
+++ b/solution.py
@@ -15,6 +15,7 @@
 W = D // TP
 HID = 224
 EXTRA = 8
+FRONT = ROWS + EXTRA
 EPS = 1e-05
 
 F32 = jnp.float32
@@ -76,7 +77,8 @@
     gain_out_ref[...] = parts.astype(BF16)
 
 
-def prepare_kernel(place_ref, weight_ref, pick_ref, weight_out_ref):
+def prepare_kernel(place_ref, weight_ref, gate_ref, up_ref, pick_ref, weight_out_ref):
+    del gate_ref, up_ref
     spots = lax.broadcasted_iota(jnp.int32, (TOK, ROWS), 1).astype(F32)
     for k in range(2):
         place = jnp.broadcast_to(place_ref[k : k + 1].astype(F32), (TOK, TOK)).T
@@ -84,36 +86,40 @@
         weight_out_ref[k] = jnp.broadcast_to(weight_ref[k : k + 1], (TOK, TOK)).T
 
 
-def spread_kernel(rows_ref, gain_ref, out_ref):
+def spread_kernel(rows_ref, gain_ref, down_ref, out_ref):
     gain = gain_ref[...]
     for block in range(CAP // 2):
         piece = rows_ref[:, :, block * W : (block + 1) * W].reshape(64, W)
         for peer in range(TP):
             out_ref[peer, block * 64 : (block + 1) * 64] = piece
     for peer in range(TP):
-        out_ref[peer, ROWS : ROWS + EXTRA] = gain
-
-
-def experts_kernel(x_ref, gate_a, gate_b, up_a, up_b, down_a, down_b, out_ref, normed_ref):
+        out_ref[peer, ROWS:FRONT] = gain
+        out_ref[peer, FRONT:] = down_ref[peer]
+
+
+def hidden_kernel(x_ref, gate_a, gate_b, up_a, up_b, out_ref, normed_ref):
     total = jnp.zeros((ROWS, W), F32)
     for t in range(TP):
         piece = x_ref[t, :ROWS].astype(F32)
         total = total + piece * piece
     scale = lax.rsqrt(jnp.sum(total, axis=1, keepdims=True) / D + EPS)
     for t in range(TP):
-        gain = jnp.sum(x_ref[t, ROWS : ROWS + EXTRA].astype(F32), axis=0, keepdims=True)
+        gain = jnp.sum(x_ref[t, ROWS:FRONT].astype(F32), axis=0, keepdims=True)
         piece = x_ref[t, :ROWS].astype(F32)
         normed_ref[:, t * W : (t + 1) * W] = (piece * scale * gain).astype(BF16)
     normed = normed_ref[...]
-    hidden = []
     across = (((1,), (1,)), ((), ()))
-    for gate_ref, up_ref in ((gate_a, up_a), (gate_b, up_b)):
+    for half, (gate_ref, up_ref) in enumerate(((gate_a, up_a), (gate_b, up_b))):
         gate = lax.dot_general(normed, gate_ref[...], across, preferred_element_type=F32)
         upper = lax.dot_general(normed, up_ref[...], across, preferred_element_type=F32)
-        hidden.append((jax.nn.silu(gate) * upper).astype(BF16))
-    for t in range(TP):
-        part = jnp.dot(hidden[0], down_a[t], preferred_element_type=F32)
-        part = part + jnp.dot(hidden[1], down_b[t], preferred_element_type=F32)
+        out_ref[half] = (jax.nn.silu(gate) * upper).astype(BF16)
+
+
+def output_kernel(hidden_ref, x_ref, down_ref, out_ref):
+    first, second = hidden_ref[0], hidden_ref[1]
+    for t in range(TP):
+        part = jnp.dot(first, x_ref[t, FRONT:], preferred_element_type=F32)
+        part = part + jnp.dot(second, down_ref[t], preferred_element_type=F32)
         out_ref[t] = part.astype(BF16)
 
 
@@ -162,23 +168,28 @@
         4,
     )(routing.T, tokens, norm_gain.reshape(1, W))
     arrived = lax.all_to_all(outgoing, "z", 0, 0, tiled=True)
-    down_own = lax.all_to_all(down_weight.reshape(TP, HID, W), "t", 0, 0, tiled=True)
     gate_other = lax.ppermute(gate_own, "c", swap)
     up_other = lax.ppermute(up_own, "c", swap)
-    down_other = lax.ppermute(down_own, "c", swap)
     pick, weight = call(
         prepare_kernel,
         [((2, TOK, ROWS), BF16), ((2, TOK, W), F32)],
         4,
-    )(place, route_weight.T)
-    spread = call(spread_kernel, ((TP, ROWS + EXTRA, W), BF16), 4)(arrived, gain_parts)
+        free=2,
+    )(place, route_weight.T, gate_other, up_other)
+    spread = call(spread_kernel, ((TP, FRONT + HID, W), BF16), 4)(
+        arrived, gain_parts, down_weight.reshape(TP, HID, W)
+    )
     features = lax.all_to_all(spread, "t", 0, 0, tiled=True)
-    parts = call(
-        experts_kernel,
-        ((TP, ROWS, W), BF16),
-        24,
+    down_other = lax.ppermute(features[:, FRONT:], "c", swap)
+    hidden = call(
+        hidden_kernel,
+        ((2, ROWS, HID), BF16),
+        16,
         scratch_shapes=[pltpu.VMEM((ROWS, D), BF16)],
-    )(features, gate_own, gate_other, up_own, up_other, down_own, down_other)
+    )(features, gate_own, gate_other, up_own, up_other)
+    parts = call(output_kernel, ((TP, ROWS, W), BF16), 8)(
+        hidden, features, down_other
+    )
     parts = lax.all_to_all(parts, "t", 0, 0, tiled=True)
     reduced = call(reduce_kernel, ((EXPERTS, 2, 640), BF16), 4)(parts)
     returned = lax.all_to_all(reduced, "z", 0, 0, tiled=True)

time: 175 us -> 174 us (level)
  starting transfers between devices: 27.2 us -> 20.1 us
  blocking collectives: 85.6 us -> 92.2 us
  local copies, waits for them, and re-layouts: 10.2 us -> 5.35 us
  waiting for transfers between devices: 44.1 us -> 48.7 us
    all_to_all x1, waiting for transfers between devices: 6.98 us -> 22.5 us  [shards(): features = lax.all_to_all(spread, 't', 0, 0, tiled=True)]
    all_to_all x1 -> x0, waiting for transfers between devices: 11.1 us -> none  [shards(): lax.all_to_all(down_weight.reshape(TP, HID, W), 't', 0, 0, tiled=True)]
    all_to_all x1 -> x0, starting transfers between devices: 7.48 us -> none  [shards(): lax.all_to_all(down_weight.reshape(TP, HID, W), 't', 0, 0, tiled=True)]
    all_to_all x1, blocking collectives: 19.4 us -> 25.4 us  [shards(): parts = lax.all_to_all(parts, 't', 0, 0, tiled=True)]
    unnamed x27 -> x19, local copies, waits for them, and re-layouts: 10.2 us -> 5.29 us
    all_to_all x1, starting transfers between devices: 4.89 us -> 7.48 us  [shards(): features = lax.all_to_all(spread, 't', 0, 0, tiled=True)]
    all_to_all x1, starting transfers between devices: 8.58 us -> 6.25 us  [shards(): returned = lax.all_to_all(reduced, 'z', 0, 0, tiled=True)]
    pallas_call x7 -> x8, Pallas kernels: 6.52 us -> 6.7 us  [run(): pl.pallas_call(kernel, out_shape=[pltpu.VMEM(s, d) for s, d in outs] if m...]
  transfers between devices with their start and end apart: 6 -> 5, of which waited for: 4 -> 2; matrix products, arithmetic and copies ran while one was open for 0% -> 0% of each run, Pallas kernels for 1% -> 2%
where the time goes in v3:
time: 174 us; the launch traced here: 173 us
  blocking collectives  92.2 us (53%)
  waiting for transfers between devices  48.7 us (28%)
  starting transfers between devices  20.1 us (12%)
  Pallas kernels  6.7 us (4%)
  local copies, waits for them, and re-layouts  5.35 us (3%)
    all_to_all x1, blocking collectives, shards(): arrived = lax.all_to_all(outgoing, 'z', 0, 0, tiled=True)  55.8 us
    all_to_all x1, waiting for transfers between devices, shards(): returned = lax.all_to_all(reduced, 'z', 0, 0, tiled=True)  26.2 us
    all_to_all x1, blocking collectives, shards(): parts = lax.all_to_all(parts, 't', 0, 0, tiled=True)  25.4 us
    all_to_all x1, waiting for transfers between devices, shards(): features = lax.all_to_all(spread, 't', 0, 0, tiled=True)  22.5 us
    all_to_all x1, blocking collectives, shards(): squares = lax.all_to_all(square, 't', 0, 0, tiled=True)  11 us
    all_to_all x1, starting transfers between devices, shards(): features = lax.all_to_all(spread, 't', 0, 0, tiled=True)  7.48 us
    pallas_call x8, Pallas kernels, run(): pl.pallas_call(kernel, out_shape=[pltpu.VMEM(s, d) for s, d in outs] if m...  6.7 us
    all_to_all x1, starting transfers between devices, shards(): returned = lax.all_to_all(reduced, 'z', 0, 0, tiled=True)  6.25 us
  transfers between devices with their start and end apart: 5, of which 2 were waited for; matrix products, arithmetic and copies ran while one was open for 0% of the time, Pallas kernels for 2%

profile of v3, /device:TPU:2, one launch (start us, length us, event | category | flops | bytes accessed | tf_op | source)
XLA Modules:
  0.0 173.2 jit_solution(9897215277363123188)
XLA Ops:
  0.0 0.8 copy-done.4
  0.8 0.7 copy-done.6
  1.4 0.7 copy-done.7
  2.1 0.3 shard_map.82
  2.4 55.8 %all_to_all.25.rows_ref = bf16[32,2,640]{2,1,0:T(2,128)(2,1)S(1)} all-to-all(bf16[32,2,640]{2,1,0:T(2,128)(2,1)S(1)} %get-tuple-element.12), channel_id=1, replica_groups=mesh['z'=32,'c'=2,'t'=16] {'z'}, dimensions={0} | all-to-all | bytes 163840 | tf_op jit(solution)/shard_map/all_to_all | solution.py:170
  58.2 1.2 copy-done.3
  59.4 0.4 shard_map.83
  59.8 0.0 copy-start
  59.8 1.4 copy-done
  61.2 7.5 %all-to-all-start.1 = ((bf16[16,552,128]{2,1,0:T(8,128)(2,1)}), bf16[16,552,128]{2,1,0:T(8,128)(2,1)S(1)}, u32[]{:S(2)}, u32[]{:S(2)}) async-start(bf16[16,552,128]{2,1,0:T(8,128)(2,1)} %copy-done), calls=%async_computation.1 | async-start | bytes 4521984 | tf_op jit(solution)/shard_map/all_to_all | solution.py:182
  68.7 1.9 %collective-permute-start = (bf16[224,2048]{1,0:T(8,128)(2,1)}, bf16[224,2048]{1,0:T(8,128)(2,1)S(1)}, u32[]{:S(2)}, u32[]{:S(2)}) collective-permute-start(bf16[224,2048]{1,0:T(8,128)(2,1)} %bitcast.11), channel_id=1, source_target_pairs={{0,16},{16,0},{1,17},{17,1},{2,18},{18,2},{3,19},{19,3},{4,20},{20... | collective-permute-start | bytes 2752520 | tf_op jit(solution)/shard_map/ppermute | solution.py:171
  70.6 2.4 %collective-permute-start.1 = (bf16[224,2048]{1,0:T(8,128)(2,1)}, bf16[224,2048]{1,0:T(8,128)(2,1)}, u32[]{:S(2)}, u32[]{:S(2)}) collective-permute-start(bf16[224,2048]{1,0:T(8,128)(2,1)} %bitcast.13), channel_id=1, source_target_pairs={{0,16},{16,0},{1,17},{17,1},{2,18},{18,2},{3,19},{19,3},{4,20},{20... | collective-permute-start | bytes 2752520 | tf_op jit(solution)/shard_map/ppermute | solution.py:172
  73.0 22.5 %all-to-all-done.1.x_ref = bf16[16,552,128]{2,1,0:T(8,128)(2,1)S(1)} async-done(((bf16[16,552,128]{2,1,0:T(8,128)(2,1)}), bf16[16,552,128]{2,1,0:T(8,128)(2,1)S(1)}, u32[]{:S(2)}, u32[]{:S(2)}) %all-to-all-start.1) | async-done | bytes 2261024 | tf_op jit(solution)/shard_map/all_to_all | solution.py:182
  95.5 0.1 slice.4
  95.5 2.1 %collective-permute-start.2 = (bf16[16,224,128]{2,1,0:T(8,128)(2,1)S(1)}, bf16[16,224,128]{2,1,0:T(8,128)(2,1)S(1)}, u32[]{:S(2)}, u32[]{:S(2)}) collective-permute-start(bf16[16,224,128]{2,1,0:T(8,128)(2,1)S(1)} %slice.4), channel_id=1, source_target_pairs={{0,16},{16,0},{1,17},{17,1},{2,18},{18,2},{3,19},{19,3},{4,20},{20... | collective-permute-start | bytes 2752520 | tf_op jit(solution)/shard_map/ppermute | solution.py:183
  97.6 0.0 collective-permute-done.gate_b.gate_ref
  97.6 0.0 collective-permute-done.1.up_b.up_ref
  97.6 0.0 copy-done.1
  97.6 3.0 %shard_map.84.hidden_ref = bf16[2,320,224]{2,1,0:T(8,128)(2,1)S(1)} custom-call(bf16[16,552,128]{2,1,0:T(8,128)(2,1)S(1)} %all-to-all-done.1.x_ref, bf16[224,2048]{1,0:T(8,128)(2,1)S(1)} %bitcast.12, bf16[224,2048]{1,0:T(8,128)(2,1)S(1)} %collective-permute-done.gate_b.gate_ref, bf16[224,2048]{1,0:T(8,128)(2,1)S(1)} %bitcast.14, ...), custom_call_target="tpu_custom_call" | custom-call | tf_op jit(solution)/shard_map/pallas_call | solution.py:32
  100.6 0.0 collective-permute-done.2.down_ref
  100.6 1.5 shard_map.85
  102.1 0.0 copy-start.5
  102.2 25.4 %all_to_all.26.parts_ref = bf16[16,320,128]{2,1,0:T(8,128)(2,1)S(1)} all-to-all(bf16[16,320,128]{2,1,0:T(8,128)(2,1)S(1)} %shard_map.85), channel_id=1, replica_groups=mesh['z'=32,'c'=2,'t'=16] {'t'}, dimensions={0} | all-to-all | bytes 2621440 | tf_op jit(solution)/shard_map/all_to_all | solution.py:193
  127.6 0.9 shard_map.86
  128.5 6.3 %all-to-all-start.3 = ((bf16[32,2,640]{2,1,0:T(2,128)(2,1)}), bf16[32,2,640]{2,1,0:T(2,128)(2,1)S(1)}, u32[]{:S(2)}, u32[]{:S(2)}) async-start(bf16[32,2,640]{2,1,0:T(2,128)(2,1)} %shard_map.86), calls=%async_computation.3 | async-start | bytes 163840 | tf_op jit(solution)/shard_map/all_to_all | solution.py:195
  134.7 0.0 copy-done.5
  134.7 0.2 shard_map.87
  135.0 26.2 %all-to-all-done.3.rows_ref = bf16[32,2,640]{2,1,0:T(2,128)(2,1)S(1)} async-done(((bf16[32,2,640]{2,1,0:T(2,128)(2,1)}), bf16[32,2,640]{2,1,0:T(2,128)(2,1)S(1)}, u32[]{:S(2)}, u32[]{:S(2)}) %all-to-all-start.3) | async-done | bytes 81952 | tf_op jit(solution)/shard_map/all_to_all | solution.py:195
  161.2 0.3 shard_map.88
  161.5 11.0 %all_to_all.27.square_ref = f32[16,1,128]{2,1,0:T(1,128)S(1)} all-to-all(f32[16,1,128]{2,1,0:T(1,128)S(1)} %get-tuple-element.18), channel_id=1, replica_groups=mesh['z'=32,'c'=2,'t'=16] {'t'}, dimensions={0} | all-to-all | bytes 16384 | tf_op jit(solution)/shard_map/all_to_all | solution.py:199
  172.5 0.1 shard_map.89
  172.6 0.6 copy.9
  (9 shorter events, 0.0 us)
Async XLA Ops:
  0.0 0.8 copy-start.4
  0.8 0.7 copy-start.6
  1.4 0.7 copy-start.7
  58.2 1.2 copy-start.3
  59.8 1.4 copy-start
  61.2 34.3 %all-to-all-start.1 = ((bf16[16,552,128]{2,1,0:T(8,128)(2,1)}), bf16[16,552,128]{2,1,0:T(8,128)(2,1)S(1)}, u32[]{:S(2)}, u32[]{:S(2)}) async-start(bf16[16,552,128]{2,1,0:T(8,128)(2,1)} %copy-done), calls=%async_computation.1 | async-start | bytes 4521984 | tf_op jit(solution)/shard_map/all_to_all | solution.py:182
  68.7 29.0 %collective-permute-start = (bf16[224,2048]{1,0:T(8,128)(2,1)}, bf16[224,2048]{1,0:T(8,128)(2,1)S(1)}, u32[]{:S(2)}, u32[]{:S(2)}) collective-permute-start(bf16[224,2048]{1,0:T(8,128)(2,1)} %bitcast.11), channel_id=1, source_target_pairs={{0,16},{16,0},{1,17},{17,1},{2,18},{18,2},{3,19},{19,3},{4,20},{20... | collective-permute-start | bytes 2752520 | tf_op jit(solution)/shard_map/ppermute | solution.py:171
  70.6 27.0 %collective-permute-start.1 = (bf16[224,2048]{1,0:T(8,128)(2,1)}, bf16[224,2048]{1,0:T(8,128)(2,1)}, u32[]{:S(2)}, u32[]{:S(2)}) collective-permute-start(bf16[224,2048]{1,0:T(8,128)(2,1)} %bitcast.13), channel_id=1, source_target_pairs={{0,16},{16,0},{1,17},{17,1},{2,18},{18,2},{3,19},{19,3},{4,20},{20... | collective-permute-start | bytes 2752520 | tf_op jit(solution)/shard_map/ppermute | solution.py:172
  95.5 2.2 %copy-start.1 = (bf16[1,2048,224]{1,2,0:T(8,128)(2,1)S(1)}, bf16[1,2048,224]{1,2,0:T(8,128)(2,1)}, u32[]{:S(2)}) copy-start(bf16[1,2048,224]{1,2,0:T(8,128)(2,1)} %param.12) | copy-start | bytes 2752516
  95.5 2.2 %copy-start.2 = (bf16[1,2048,224]{1,2,0:T(8,128)(2,1)S(1)}, bf16[1,2048,224]{1,2,0:T(8,128)(2,1)}, u32[]{:S(2)}) copy-start(bf16[1,2048,224]{1,2,0:T(8,128)(2,1)} %param.13) | copy-start | bytes 2752516
  95.5 5.1 %collective-permute-start.2 = (bf16[16,224,128]{2,1,0:T(8,128)(2,1)S(1)}, bf16[16,224,128]{2,1,0:T(8,128)(2,1)S(1)}, u32[]{:S(2)}, u32[]{:S(2)}) collective-permute-start(bf16[16,224,128]{2,1,0:T(8,128)(2,1)S(1)} %slice.4), channel_id=1, source_target_pairs={{0,16},{16,0},{1,17},{17,1},{2,18},{18,2},{3,19},{19,3},{4,20},{20... | collective-permute-start | bytes 2752520 | tf_op jit(solution)/shard_map/ppermute | solution.py:183
  102.1 32.6 %copy-start.5 = (f32[128,2]{0,1:T(2,128)S(1)}, f32[128,2]{0,1:T(2,128)}, u32[]{:S(2)}) copy-start(f32[128,2]{0,1:T(2,128)} %param.11) | copy-start | bytes 3076
  127.6 44.9 %copy-start.8 = (f32[128]{0:T(128)S(1)}, f32[128]{0:T(128)}, u32[]{:S(2)}) copy-start(f32[128]{0:T(128)} %param.15) | copy-start | bytes 1540
  128.5 32.7 %all-to-all-start.3 = ((bf16[32,2,640]{2,1,0:T(2,128)(2,1)}), bf16[32,2,640]{2,1,0:T(2,128)(2,1)S(1)}, u32[]{:S(2)}, u32[]{:S(2)}) async-start(bf16[32,2,640]{2,1,0:T(2,128)(2,1)} %shard_map.86), calls=%async_computation.3 | async-start | bytes 163840 | tf_op jit(solution)/shard_map/all_to_all | solution.py:195

commit v4 on v3

--- a/solution.py
+++ b/solution.py
@@ -77,8 +77,7 @@
     gain_out_ref[...] = parts.astype(BF16)
 
 
-def prepare_kernel(place_ref, weight_ref, gate_ref, up_ref, pick_ref, weight_out_ref):
-    del gate_ref, up_ref
+def prepare_kernel(place_ref, weight_ref, pick_ref, weight_out_ref):
     spots = lax.broadcasted_iota(jnp.int32, (TOK, ROWS), 1).astype(F32)
     for k in range(2):
         place = jnp.broadcast_to(place_ref[k : k + 1].astype(F32), (TOK, TOK)).T
@@ -86,7 +85,7 @@
         weight_out_ref[k] = jnp.broadcast_to(weight_ref[k : k + 1], (TOK, TOK)).T
 
 
-def spread_kernel(rows_ref, gain_ref, down_ref, out_ref):
+def spread_kernel(rows_ref, gain_ref, out_ref):
     gain = gain_ref[...]
     for block in range(CAP // 2):
         piece = rows_ref[:, :, block * W : (block + 1) * W].reshape(64, W)
@@ -94,10 +93,17 @@
             out_ref[peer, block * 64 : (block + 1) * 64] = piece
     for peer in range(TP):
         out_ref[peer, ROWS:FRONT] = gain
-        out_ref[peer, FRONT:] = down_ref[peer]
-
-
-def hidden_kernel(x_ref, gate_a, gate_b, up_a, up_b, out_ref, normed_ref):
+
+
+def hidden_kernel(
+    x_ref, gate_a, up_a, gate_far, up_far, out_ref, normed_ref, gate_b, up_b, sems
+):
+    copies = [
+        pltpu.make_async_copy(gate_far, gate_b, sems.at[0]),
+        pltpu.make_async_copy(up_far, up_b, sems.at[1]),
+    ]
+    for copy in copies:
+        copy.start()
     total = jnp.zeros((ROWS, W), F32)
     for t in range(TP):
         piece = x_ref[t, :ROWS].astype(F32)
@@ -109,17 +115,23 @@
         normed_ref[:, t * W : (t + 1) * W] = (piece * scale * gain).astype(BF16)
     normed = normed_ref[...]
     across = (((1,), (1,)), ((), ()))
-    for half, (gate_ref, up_ref) in enumerate(((gate_a, up_a), (gate_b, up_b))):
+
+    def half(gate_ref, up_ref):
         gate = lax.dot_general(normed, gate_ref[...], across, preferred_element_type=F32)
         upper = lax.dot_general(normed, up_ref[...], across, preferred_element_type=F32)
-        out_ref[half] = (jax.nn.silu(gate) * upper).astype(BF16)
-
-
-def output_kernel(hidden_ref, x_ref, down_ref, out_ref):
+        return (jax.nn.silu(gate) * upper).astype(BF16)
+
+    out_ref[0] = half(gate_a, up_a)
+    for copy in copies:
+        copy.wait()
+    out_ref[1] = half(gate_b, up_b)
+
+
+def output_kernel(hidden_ref, down_a, down_b, out_ref):
     first, second = hidden_ref[0], hidden_ref[1]
     for t in range(TP):
-        part = jnp.dot(first, x_ref[t, FRONT:], preferred_element_type=F32)
-        part = part + jnp.dot(second, down_ref[t], preferred_element_type=F32)
+        part = jnp.dot(first, down_a[t], preferred_element_type=F32)
+        part = part + jnp.dot(second, down_b[t], preferred_element_type=F32)
         out_ref[t] = part.astype(BF16)
 
 
@@ -168,27 +180,31 @@
         4,
     )(routing.T, tokens, norm_gain.reshape(1, W))
     arrived = lax.all_to_all(outgoing, "z", 0, 0, tiled=True)
+    down_own = lax.all_to_all(down_weight.reshape(TP, HID, W), "t", 0, 0, tiled=True)
     gate_other = lax.ppermute(gate_own, "c", swap)
     up_other = lax.ppermute(up_own, "c", swap)
+    down_other = lax.ppermute(down_own, "c", swap)
     pick, weight = call(
         prepare_kernel,
         [((2, TOK, ROWS), BF16), ((2, TOK, W), F32)],
         4,
-        free=2,
-    )(place, route_weight.T, gate_other, up_other)
-    spread = call(spread_kernel, ((TP, FRONT + HID, W), BF16), 4)(
-        arrived, gain_parts, down_weight.reshape(TP, HID, W)
-    )
+    )(place, route_weight.T)
+    spread = call(spread_kernel, ((TP, FRONT, W), BF16), 4)(arrived, gain_parts)
     features = lax.all_to_all(spread, "t", 0, 0, tiled=True)
-    down_other = lax.ppermute(features[:, FRONT:], "c", swap)
     hidden = call(
         hidden_kernel,
         ((2, ROWS, HID), BF16),
         16,
-        scratch_shapes=[pltpu.VMEM((ROWS, D), BF16)],
-    )(features, gate_own, gate_other, up_own, up_other)
+        free=2,
+        scratch_shapes=[
+            pltpu.VMEM((ROWS, D), BF16),
+            pltpu.VMEM((HID, D), BF16),
+            pltpu.VMEM((HID, D), BF16),
+            pltpu.SemaphoreType.DMA((2,)),
+        ],
+    )(features, gate_own, up_own, gate_other, up_other)
     parts = call(output_kernel, ((TP, ROWS, W), BF16), 8)(
-        hidden, features, down_other
+        hidden, down_own, down_other
     )
     parts = lax.all_to_all(parts, "t", 0, 0, tiled=True)
     reduced = call(reduce_kernel, ((EXPERTS, 2, 640), BF16), 4)(parts)

time: 174 us -> 175 us (level)
  starting transfers between devices: 20.1 us -> 27.2 us
  blocking collectives: 92.2 us -> 85.7 us
  waiting for transfers between devices: 48.7 us -> 45 us
  local copies, waits for them, and re-layouts: 5.35 us -> 8.15 us
    all_to_all x1, waiting for transfers between devices: 22.5 us -> 8.43 us  [shards(): features = lax.all_to_all(spread, 't', 0, 0, tiled=True)]
    all_to_all x0 -> x1, waiting for transfers between devices: none -> 11.1 us  [shards(): lax.all_to_all(down_weight.reshape(TP, HID, W), 't', 0, 0, tiled=True)]
    all_to_all x0 -> x1, starting transfers between devices: none -> 7.48 us  [shards(): lax.all_to_all(down_weight.reshape(TP, HID, W), 't', 0, 0, tiled=True)]
    all_to_all x1, blocking collectives: 25.4 us -> 19.4 us  [shards(): parts = lax.all_to_all(parts, 't', 0, 0, tiled=True)]
    unnamed x19 -> x23, local copies, waits for them, and re-layouts: 5.29 us -> 8.15 us
    all_to_all x1, starting transfers between devices: 7.48 us -> 4.89 us  [shards(): features = lax.all_to_all(spread, 't', 0, 0, tiled=True)]
    all_to_all x1, starting transfers between devices: 6.25 us -> 8.56 us  [shards(): returned = lax.all_to_all(reduced, 'z', 0, 0, tiled=True)]
  transfers between devices with their start and end apart: 5 -> 6, of which waited for: 2 -> 3; matrix products, arithmetic and copies ran while one was open for 0% -> 0% of each run, Pallas kernels for 2% -> 2%
where the time goes in v4:
time: 175 us
  blocking collectives  85.7 us (49%)
  waiting for transfers between devices  45 us (26%)
  starting transfers between devices  27.2 us (16%)
  Pallas kernels  8.43 us (5%)
  local copies, waits for them, and re-layouts  8.15 us (5%)
    all_to_all x1, blocking collectives, shards(): arrived = lax.all_to_all(outgoing, 'z', 0, 0, tiled=True)  55.8 us
    all_to_all x1, waiting for transfers between devices, shards(): returned = lax.all_to_all(reduced, 'z', 0, 0, tiled=True)  25.4 us
    all_to_all x1, blocking collectives, shards(): parts = lax.all_to_all(parts, 't', 0, 0, tiled=True)  19.4 us
    all_to_all x1, waiting for transfers between devices, shards(): lax.all_to_all(down_weight.reshape(TP, HID, W), 't', 0, 0, tiled=True)  11.1 us
    all_to_all x1, blocking collectives, shards(): squares = lax.all_to_all(square, 't', 0, 0, tiled=True)  10.5 us
    all_to_all x1, starting transfers between devices, shards(): returned = lax.all_to_all(reduced, 'z', 0, 0, tiled=True)  8.56 us
    all_to_all x1, waiting for transfers between devices, shards(): features = lax.all_to_all(spread, 't', 0, 0, tiled=True)  8.43 us
    pallas_call x8, Pallas kernels, run(): pl.pallas_call(kernel, out_shape=[pltpu.VMEM(s, d) for s, d in outs] if m...  8.43 us
  transfers between devices with their start and end apart: 6, of which 3 were waited for; matrix products, arithmetic and copies ran while one was open for 0% of the time, Pallas kernels for 2%

profile of v4, /device:TPU:2, one launch (start us, length us, event | category | flops | bytes accessed | tf_op | source)
XLA Modules:
  0.0 174.6 jit_solution(1560580786999291221)
XLA Ops:
  0.0 0.8 copy-done.6
  0.8 0.7 copy-done.7
  1.4 0.7 copy-done.9
  2.1 0.3 shard_map.82
  2.4 55.8 %all_to_all.30.rows_ref = bf16[32,2,640]{2,1,0:T(2,128)(2,1)S(1)} all-to-all(bf16[32,2,640]{2,1,0:T(2,128)(2,1)S(1)} %get-tuple-element.12), channel_id=1, replica_groups=mesh['z'=32,'c'=2,'t'=16] {'z'}, dimensions={0} | all-to-all | bytes 163840 | tf_op jit(solution)/shard_map/all_to_all | solution.py:182
  58.2 7.5 %all-to-all-start.2 = ((bf16[16,224,128]{2,1,0:T(8,128)(2,1)}), bf16[16,224,128]{2,1,0:T(8,128)(2,1)S(1)}, u32[]{:S(2)}, u32[]{:S(2)}) async-start(bf16[16,224,128]{2,1,0:T(8,128)(2,1)} %bitcast.19), calls=%async_computation.2 | async-start | bytes 1835008 | tf_op jit(solution)/shard_map/all_to_all | solution.py:183
  65.7 1.4 shard_map.83
  67.2 11.1 %all-to-all-done.2.down_a = bf16[16,224,128]{2,1,0:T(8,128)(2,1)S(1)} async-done(((bf16[16,224,128]{2,1,0:T(8,128)(2,1)}), bf16[16,224,128]{2,1,0:T(8,128)(2,1)S(1)}, u32[]{:S(2)}, u32[]{:S(2)}) %all-to-all-start.2) | async-done | bytes 917536 | tf_op jit(solution)/shard_map/all_to_all | solution.py:183
  78.3 4.9 %all-to-all-start.1 = ((bf16[16,328,128]{2,1,0:T(8,128)(2,1)}), bf16[16,328,128]{2,1,0:T(8,128)(2,1)S(1)}, u32[]{:S(2)}, u32[]{:S(2)}) async-start(bf16[16,328,128]{2,1,0:T(8,128)(2,1)} %shard_map.83), calls=%async_computation.1 | async-start | bytes 2686976 | tf_op jit(solution)/shard_map/all_to_all | solution.py:193
  83.2 1.9 %collective-permute-start = (bf16[224,2048]{1,0:T(8,128)(2,1)S(1)}, bf16[224,2048]{1,0:T(8,128)(2,1)S(1)}, u32[]{:S(2)}, u32[]{:S(2)}) collective-permute-start(bf16[224,2048]{1,0:T(8,128)(2,1)S(1)} %bitcast.11), channel_id=1, source_target_pairs={{0,16},{16,0},{1,17},{17,1},{2,18},{18,2},{3,19},{19,3},{4,20},{20... | collective-permute-start | bytes 2752520 | tf_op jit(solution)/shard_map/ppermute | solution.py:184
  85.1 2.4 %collective-permute-start.1 = (bf16[224,2048]{1,0:T(8,128)(2,1)}, bf16[224,2048]{1,0:T(8,128)(2,1)S(1)}, u32[]{:S(2)}, u32[]{:S(2)}) collective-permute-start(bf16[224,2048]{1,0:T(8,128)(2,1)} %bitcast.13), channel_id=1, source_target_pairs={{0,16},{16,0},{1,17},{17,1},{2,18},{18,2},{3,19},{19,3},{4,20},{20... | collective-permute-start | bytes 2752520 | tf_op jit(solution)/shard_map/ppermute | solution.py:185
  87.5 1.9 %collective-permute-start.2 = (bf16[16,224,128]{2,1,0:T(8,128)(2,1)S(1)}, bf16[16,224,128]{2,1,0:T(8,128)(2,1)}, u32[]{:S(2)}, u32[]{:S(2)}) collective-permute-start(bf16[16,224,128]{2,1,0:T(8,128)(2,1)S(1)} %all-to-all-done.2.down_a), channel_id=1, source_target_pairs={{0,16},{16,0},{1,17},{17,1},{2,18},{18,2},{3,19},{19,3},{4,20},{20... | collective-permute-start | bytes 2752520 | tf_op jit(solution)/shard_map/ppermute | solution.py:186
  89.5 0.0 collective-permute-done.gate_far
  89.5 0.9 copy-done.2
  90.4 0.0 collective-permute-done.1.up_far
  90.4 1.0 copy-done.4
  91.4 8.4 %all-to-all-done.1.x_ref = bf16[16,328,128]{2,1,0:T(8,128)(2,1)S(1)} async-done(((bf16[16,328,128]{2,1,0:T(8,128)(2,1)}), bf16[16,328,128]{2,1,0:T(8,128)(2,1)S(1)}, u32[]{:S(2)}, u32[]{:S(2)}) %all-to-all-start.1) | async-done | bytes 1343520 | tf_op jit(solution)/shard_map/all_to_all | solution.py:193
  99.8 1.2 copy-done.1
  101.0 1.2 copy-done.3
  102.2 1.2 copy-done.5
  103.4 2.5 %shard_map.84.hidden_ref = bf16[2,320,224]{2,1,0:T(8,128)(2,1)S(1)} custom-call(bf16[16,328,128]{2,1,0:T(8,128)(2,1)S(1)} %all-to-all-done.1.x_ref, bf16[224,2048]{1,0:T(8,128)(2,1)S(1)} %bitcast.12, bf16[224,2048]{1,0:T(8,128)(2,1)S(1)} %bitcast.14, bf16[224,2048]{1,0:T(8,128)(2,1)S(1)} %copy-done.3, bf16[224,2048]{1,0:T(8,128)(2,1)S(1)} %copy-done.5), custom_call_target="tpu_custom_call" | custom-call | tf_op jit(solution)/shard_map/pallas_call | solution.py:32
  105.8 0.0 collective-permute-done.2.down_b
  105.8 2.7 %shard_map.85 = bf16[16,320,128]{2,1,0:T(8,128)(2,1)S(1)} custom-call(bf16[2,320,224]{2,1,0:T(8,128)(2,1)S(1)} %shard_map.84.hidden_ref, bf16[16,224,128]{2,1,0:T(8,128)(2,1)S(1)} %all-to-all-done.2.down_a, bf16[16,224,128]{2,1,0:T(8,128)(2,1)} %collective-permute-done.2.down_b), custom_call_target="tpu_custom_call" | custom-call | tf_op jit(solution)/shard_map/pallas_call | solution.py:32
  108.5 19.4 %all_to_all.31.parts_ref = bf16[16,320,128]{2,1,0:T(8,128)(2,1)S(1)} all-to-all(bf16[16,320,128]{2,1,0:T(8,128)(2,1)S(1)} %shard_map.85), channel_id=1, replica_groups=mesh['z'=32,'c'=2,'t'=16] {'t'}, dimensions={0} | all-to-all | bytes 2621440 | tf_op jit(solution)/shard_map/all_to_all | solution.py:209
  127.9 0.8 shard_map.86
  128.8 8.6 %all-to-all-start.4 = ((bf16[32,2,640]{2,1,0:T(2,128)(2,1)}), bf16[32,2,640]{2,1,0:T(2,128)(2,1)S(1)}, u32[]{:S(2)}, u32[]{:S(2)}) async-start(bf16[32,2,640]{2,1,0:T(2,128)(2,1)} %shard_map.86), calls=%async_computation.4 | async-start | bytes 163840 | tf_op jit(solution)/shard_map/all_to_all | solution.py:211
  137.4 0.2 shard_map.87
  137.6 25.4 %all-to-all-done.4.rows_ref = bf16[32,2,640]{2,1,0:T(2,128)(2,1)S(1)} async-done(((bf16[32,2,640]{2,1,0:T(2,128)(2,1)}), bf16[32,2,640]{2,1,0:T(2,128)(2,1)S(1)}, u32[]{:S(2)}, u32[]{:S(2)}) %all-to-all-start.4) | async-done | bytes 81952 | tf_op jit(solution)/shard_map/all_to_all | solution.py:211
  163.0 0.3 shard_map.88
  163.3 10.5 %all_to_all.32.square_ref = f32[16,1,128]{2,1,0:T(1,128)S(1)} all-to-all(f32[16,1,128]{2,1,0:T(1,128)S(1)} %get-tuple-element.18), channel_id=1, replica_groups=mesh['z'=32,'c'=2,'t'=16] {'t'}, dimensions={0} | all-to-all | bytes 16384 | tf_op jit(solution)/shard_map/all_to_all | solution.py:215
  173.8 0.1 shard_map.89
  173.9 0.6 copy.9
  (14 shorter events, 0.0 us)
Async XLA Ops:
  0.0 0.8 copy-start.6
  0.8 0.7 copy-start.7
  1.4 0.7 copy-start.9
  58.2 20.1 %all-to-all-start.2 = ((bf16[16,224,128]{2,1,0:T(8,128)(2,1)}), bf16[16,224,128]{2,1,0:T(8,128)(2,1)S(1)}, u32[]{:S(2)}, u32[]{:S(2)}) async-start(bf16[16,224,128]{2,1,0:T(8,128)(2,1)} %bitcast.19), calls=%async_computation.2 | async-start | bytes 1835008 | tf_op jit(solution)/shard_map/all_to_all | solution.py:183
  67.1 16.0 %copy-start = (bf16[1,2048,224]{1,2,0:T(8,128)(2,1)S(1)}, bf16[1,2048,224]{1,2,0:T(8,128)(2,1)}, u32[]{:S(2)}) copy-start(bf16[1,2048,224]{1,2,0:T(8,128)(2,1)} %param.12) | copy-start | bytes 2752516
  78.3 21.5 %all-to-all-start.1 = ((bf16[16,328,128]{2,1,0:T(8,128)(2,1)}), bf16[16,328,128]{2,1,0:T(8,128)(2,1)S(1)}, u32[]{:S(2)}, u32[]{:S(2)}) async-start(bf16[16,328,128]{2,1,0:T(8,128)(2,1)} %shard_map.83), calls=%async_computation.1 | async-start | bytes 2686976 | tf_op jit(solution)/shard_map/all_to_all | solution.py:193
  83.2 6.3 %collective-permute-start = (bf16[224,2048]{1,0:T(8,128)(2,1)S(1)}, bf16[224,2048]{1,0:T(8,128)(2,1)S(1)}, u32[]{:S(2)}, u32[]{:S(2)}) collective-permute-start(bf16[224,2048]{1,0:T(8,128)(2,1)S(1)} %bitcast.11), channel_id=1, source_target_pairs={{0,16},{16,0},{1,17},{17,1},{2,18},{18,2},{3,19},{19,3},{4,20},{20... | collective-permute-start | bytes 2752520 | tf_op jit(solution)/shard_map/ppermute | solution.py:184
  85.1 5.3 %collective-permute-start.1 = (bf16[224,2048]{1,0:T(8,128)(2,1)}, bf16[224,2048]{1,0:T(8,128)(2,1)S(1)}, u32[]{:S(2)}, u32[]{:S(2)}) collective-permute-start(bf16[224,2048]{1,0:T(8,128)(2,1)} %bitcast.13), channel_id=1, source_target_pairs={{0,16},{16,0},{1,17},{17,1},{2,18},{18,2},{3,19},{19,3},{4,20},{20... | collective-permute-start | bytes 2752520 | tf_op jit(solution)/shard_map/ppermute | solution.py:185
  87.5 18.3 %collective-permute-start.2 = (bf16[16,224,128]{2,1,0:T(8,128)(2,1)S(1)}, bf16[16,224,128]{2,1,0:T(8,128)(2,1)}, u32[]{:S(2)}, u32[]{:S(2)}) collective-permute-start(bf16[16,224,128]{2,1,0:T(8,128)(2,1)S(1)} %all-to-all-done.2.down_a), channel_id=1, source_target_pairs={{0,16},{16,0},{1,17},{17,1},{2,18},{18,2},{3,19},{19,3},{4,20},{20... | collective-permute-start | bytes 2752520 | tf_op jit(solution)/shard_map/ppermute | solution.py:186
  89.5 1.0 copy-start.2
  90.4 1.0 copy-start.4
  99.8 1.2 copy-start.1
  101.0 1.2 copy-start.3
  102.2 1.2 copy-start.5
  127.9 9.4 %copy-start.8 = (f32[128,2]{0,1:T(2,128)S(1)}, f32[128,2]{0,1:T(2,128)}, u32[]{:S(2)}) copy-start(f32[128,2]{0,1:T(2,128)} %param.11) | copy-start | bytes 3076
  127.9 45.9 %copy-start.10 = (f32[128]{0:T(128)S(1)}, f32[128]{0:T(128)}, u32[]{:S(2)}) copy-start(f32[128]{0:T(128)} %param.15) | copy-start | bytes 1540
  128.8 34.2 %all-to-all-start.4 = ((bf16[32,2,640]{2,1,0:T(2,128)(2,1)}), bf16[32,2,640]{2,1,0:T(2,128)(2,1)S(1)}, u32[]{:S(2)}, u32[]{:S(2)}) async-start(bf16[32,2,640]{2,1,0:T(2,128)(2,1)} %shard_map.86), calls=%async_computation.4 | async-start | bytes 163840 | tf_op jit(solution)/shard_map/all_to_all | solution.py:211

commit v5 on v4

--- a/solution.py
+++ b/solution.py
@@ -15,6 +15,7 @@
 W = D // TP
 HID = 224
 EXTRA = 8
+FIRST = 16
 FRONT = ROWS + EXTRA
 EPS = 1e-05
 
@@ -42,7 +43,13 @@
 
 
 def place_of(slot, expert):
-    return (slot // 2) * (2 * EXPERTS) + 2 * expert + slot % 2
+    position = (expert + EXPERTS - FIRST) % EXPERTS
+    return (slot // 2) * (2 * EXPERTS) + 2 * position + slot % 2
+
+
+def exchange(blocks):
+    order = [(p + FIRST) % EXPERTS for p in range(EXPERTS)]
+    return lax.all_to_all(blocks, "z", 0, 0, axis_index_groups=[order], tiled=True)
 
 
 def dispatch_kernel(routing_ref, tokens_ref, gain_ref, out_ref, place_ref, gain_out_ref):
@@ -85,7 +92,7 @@
         weight_out_ref[k] = jnp.broadcast_to(weight_ref[k : k + 1], (TOK, TOK)).T
 
 
-def spread_kernel(rows_ref, gain_ref, out_ref):
+def spread_kernel(rows_ref, gain_ref, down_ref, out_ref):
     gain = gain_ref[...]
     for block in range(CAP // 2):
         piece = rows_ref[:, :, block * W : (block + 1) * W].reshape(64, W)
@@ -93,6 +100,7 @@
             out_ref[peer, block * 64 : (block + 1) * 64] = piece
     for peer in range(TP):
         out_ref[peer, ROWS:FRONT] = gain
+        out_ref[peer, FRONT:] = down_ref[peer]
 
 
 def hidden_kernel(
@@ -127,11 +135,11 @@
     out_ref[1] = half(gate_b, up_b)
 
 
-def output_kernel(hidden_ref, down_a, down_b, out_ref):
+def output_kernel(hidden_ref, x_ref, down_ref, out_ref):
     first, second = hidden_ref[0], hidden_ref[1]
     for t in range(TP):
-        part = jnp.dot(first, down_a[t], preferred_element_type=F32)
-        part = part + jnp.dot(second, down_b[t], preferred_element_type=F32)
+        part = jnp.dot(first, x_ref[t, FRONT:], preferred_element_type=F32)
+        part = part + jnp.dot(second, down_ref[t], preferred_element_type=F32)
         out_ref[t] = part.astype(BF16)
 
 
@@ -179,18 +187,19 @@
         [((EXPERTS, 2, 640), BF16), ((2, TOK), jnp.int32), ((EXTRA, W), BF16)],
         4,
     )(routing.T, tokens, norm_gain.reshape(1, W))
-    arrived = lax.all_to_all(outgoing, "z", 0, 0, tiled=True)
-    down_own = lax.all_to_all(down_weight.reshape(TP, HID, W), "t", 0, 0, tiled=True)
+    arrived = exchange(outgoing)
     gate_other = lax.ppermute(gate_own, "c", swap)
     up_other = lax.ppermute(up_own, "c", swap)
-    down_other = lax.ppermute(down_own, "c", swap)
     pick, weight = call(
         prepare_kernel,
         [((2, TOK, ROWS), BF16), ((2, TOK, W), F32)],
         4,
     )(place, route_weight.T)
-    spread = call(spread_kernel, ((TP, FRONT, W), BF16), 4)(arrived, gain_parts)
+    spread = call(spread_kernel, ((TP, FRONT + HID, W), BF16), 4)(
+        arrived, gain_parts, down_weight.reshape(TP, HID, W)
+    )
     features = lax.all_to_all(spread, "t", 0, 0, tiled=True)
+    down_other = lax.ppermute(features[:, FRONT:], "c", swap)
     hidden = call(
         hidden_kernel,
         ((2, ROWS, HID), BF16),
@@ -204,11 +213,11 @@
         ],
     )(features, gate_own, up_own, gate_other, up_other)
     parts = call(output_kernel, ((TP, ROWS, W), BF16), 8)(
-        hidden, down_own, down_other
+        hidden, features, down_other
     )
     parts = lax.all_to_all(parts, "t", 0, 0, tiled=True)
     reduced = call(reduce_kernel, ((EXPERTS, 2, 640), BF16), 4)(parts)
-    returned = lax.all_to_all(reduced, "z", 0, 0, tiled=True)
+    returned = exchange(reduced)
     mixed, square = call(
         combine_kernel, [((TOK, W), F32), ((TP, 1, TOK), F32)], 4
     )(returned, pick, weight)

time: 175 us -> 161 us (0.920)
  the two profiles are of different devices: /device:TPU:2 before, /device:TPU:32 now
where the time goes in v5:
time: 161 us
  blocking collectives  77.3 us (48%)
  starting transfers between devices  36 us (22%)
  waiting for transfers between devices  36 us (22%)
  Pallas kernels  6.08 us (4%)
  local copies, waits for them, and re-layouts  5.35 us (3%)
    all_to_all x1, blocking collectives, exchange(): lax.all_to_all(blocks, 'z', 0, 0, axis_index_groups=[order], tiled=True)  43 us
    all_to_all x1, waiting for transfers between devices, shards(): features = lax.all_to_all(spread, 't', 0, 0, tiled=True)  28.2 us
    all_to_all x1, blocking collectives, shards(): parts = lax.all_to_all(parts, 't', 0, 0, tiled=True)  23.5 us
    all_to_all x1, starting transfers between devices, exchange(): lax.all_to_all(blocks, 'z', 0, 0, axis_index_groups=[order], tiled=True)  22.4 us
    all_to_all x1, blocking collectives, shards(): squares = lax.all_to_all(square, 't', 0, 0, tiled=True)  10.8 us
    all_to_all x1, waiting for transfers between devices, exchange(): lax.all_to_all(blocks, 'z', 0, 0, axis_index_groups=[order], tiled=True)  7.75 us
    all_to_all x1, starting transfers between devices, shards(): features = lax.all_to_all(spread, 't', 0, 0, tiled=True)  7.17 us
    pallas_call x8, Pallas kernels, run(): pl.pallas_call(kernel, out_shape=[pltpu.VMEM(s, d) for s, d in outs] if m...  6.08 us
  transfers between devices with their start and end apart: 5, of which 2 were waited for; matrix products, arithmetic and copies ran while one was open for 0% of the time, Pallas kernels for 2%

profile of v5, /device:TPU:32, one launch (start us, length us, event | category | flops | bytes accessed | tf_op | source)
XLA Modules:
  0.0 160.8 jit_solution(10050675962647704441)
XLA Ops:
  0.0 0.8 copy-done.4
  0.8 0.7 copy-done.5
  1.4 0.7 copy-done.7
  2.1 0.3 shard_map.82
  2.4 43.0 %all_to_all.25.rows_ref = bf16[32,2,640]{2,1,0:T(2,128)(2,1)S(1)} all-to-all(bf16[32,2,640]{2,1,0:T(2,128)(2,1)S(1)} %get-tuple-element.12), channel_id=1, replica_groups={{512,544,576,608,640,672,704,736,768,800,832,864,896,928,960,992,0,32,6..., dimensions={0} | all-to-all | bytes 163840 | tf_op jit(solution)/shard_map/all_to_all | solution.py:52
  45.4 1.2 copy-done.3
  46.6 0.4 shard_map.83
  47.0 0.0 copy-start
  47.0 1.4 copy-done
  48.4 7.2 %all-to-all-start.1 = ((bf16[16,552,128]{2,1,0:T(8,128)(2,1)}), bf16[16,552,128]{2,1,0:T(8,128)(2,1)S(1)}, u32[]{:S(2)}, u32[]{:S(2)}) async-start(bf16[16,552,128]{2,1,0:T(8,128)(2,1)} %copy-done), calls=%async_computation.1 | async-start | bytes 4521984 | tf_op jit(solution)/shard_map/all_to_all | solution.py:201
  55.5 0.0 copy-done.1
  55.6 1.9 %collective-permute-start = (bf16[224,2048]{1,0:T(8,128)(2,1)S(1)}, bf16[224,2048]{1,0:T(8,128)(2,1)}, u32[]{:S(2)}, u32[]{:S(2)}) collective-permute-start(bf16[224,2048]{1,0:T(8,128)(2,1)S(1)} %bitcast.11), channel_id=1, source_target_pairs={{0,16},{16,0},{1,17},{17,1},{2,18},{18,2},{3,19},{19,3},{4,20},{20... | collective-permute-start | bytes 2752520 | tf_op jit(solution)/shard_map/ppermute | solution.py:191
  57.5 2.4 %collective-permute-start.1 = (bf16[224,2048]{1,0:T(8,128)(2,1)}, bf16[224,2048]{1,0:T(8,128)(2,1)}, u32[]{:S(2)}, u32[]{:S(2)}) collective-permute-start(bf16[224,2048]{1,0:T(8,128)(2,1)} %bitcast.13), channel_id=1, source_target_pairs={{0,16},{16,0},{1,17},{17,1},{2,18},{18,2},{3,19},{19,3},{4,20},{20... | collective-permute-start | bytes 2752520 | tf_op jit(solution)/shard_map/ppermute | solution.py:192
  59.9 28.2 %all-to-all-done.1.x_ref = bf16[16,552,128]{2,1,0:T(8,128)(2,1)S(1)} async-done(((bf16[16,552,128]{2,1,0:T(8,128)(2,1)}), bf16[16,552,128]{2,1,0:T(8,128)(2,1)S(1)}, u32[]{:S(2)}, u32[]{:S(2)}) %all-to-all-start.1) | async-done | bytes 2261024 | tf_op jit(solution)/shard_map/all_to_all | solution.py:201
  88.1 0.1 slice.4
  88.1 2.1 %collective-permute-start.2 = (bf16[16,224,128]{2,1,0:T(8,128)(2,1)S(1)}, bf16[16,224,128]{2,1,0:T(8,128)(2,1)S(1)}, u32[]{:S(2)}, u32[]{:S(2)}) collective-permute-start(bf16[16,224,128]{2,1,0:T(8,128)(2,1)S(1)} %slice.4), channel_id=1, source_target_pairs={{0,16},{16,0},{1,17},{17,1},{2,18},{18,2},{3,19},{19,3},{4,20},{20... | collective-permute-start | bytes 2752520 | tf_op jit(solution)/shard_map/ppermute | solution.py:202
  90.2 0.0 collective-permute-done.gate_far
  90.2 0.0 collective-permute-done.1.up_far
  90.2 2.4 %shard_map.84.hidden_ref = bf16[2,320,224]{2,1,0:T(8,128)(2,1)S(1)} custom-call(bf16[16,552,128]{2,1,0:T(8,128)(2,1)S(1)} %all-to-all-done.1.x_ref, bf16[224,2048]{1,0:T(8,128)(2,1)S(1)} %bitcast.12, bf16[224,2048]{1,0:T(8,128)(2,1)S(1)} %bitcast.14, bf16[224,2048]{1,0:T(8,128)(2,1)} %collective-permute-done.gate_far, ...), custom_call_target="tpu_custom_call" | custom-call | tf_op jit(solution)/shard_map/pallas_call | solution.py:33
  92.6 0.0 collective-permute-done.2.down_ref
  92.6 1.5 shard_map.85
  94.1 0.0 copy-start.6
  94.2 0.0 copy-start.8
  94.2 23.5 %all_to_all.26.parts_ref = bf16[16,320,128]{2,1,0:T(8,128)(2,1)S(1)} all-to-all(bf16[16,320,128]{2,1,0:T(8,128)(2,1)S(1)} %shard_map.85), channel_id=1, replica_groups=mesh['z'=32,'c'=2,'t'=16] {'t'}, dimensions={0} | all-to-all | bytes 2621440 | tf_op jit(solution)/shard_map/all_to_all | solution.py:218
  117.7 0.9 shard_map.86
  118.5 22.4 %all-to-all-start.3 = ((bf16[32,2,640]{2,1,0:T(2,128)(2,1)}), bf16[32,2,640]{2,1,0:T(2,128)(2,1)S(1)}, u32[]{:S(2)}, u32[]{:S(2)}) async-start(bf16[32,2,640]{2,1,0:T(2,128)(2,1)} %shard_map.86), calls=%async_computation.3 | async-start | bytes 163840 | tf_op jit(solution)/shard_map/all_to_all | solution.py:52
  141.0 0.2 shard_map.87
  141.2 7.8 %all-to-all-done.3.rows_ref = bf16[32,2,640]{2,1,0:T(2,128)(2,1)S(1)} async-done(((bf16[32,2,640]{2,1,0:T(2,128)(2,1)}), bf16[32,2,640]{2,1,0:T(2,128)(2,1)S(1)}, u32[]{:S(2)}, u32[]{:S(2)}) %all-to-all-start.3) | async-done | bytes 81952 | tf_op jit(solution)/shard_map/all_to_all | solution.py:52
  149.0 0.3 shard_map.88
  149.3 10.8 %all_to_all.27.square_ref = f32[16,1,128]{2,1,0:T(1,128)S(1)} all-to-all(f32[16,1,128]{2,1,0:T(1,128)S(1)} %get-tuple-element.18), channel_id=1, replica_groups=mesh['z'=32,'c'=2,'t'=16] {'t'}, dimensions={0} | all-to-all | bytes 16384 | tf_op jit(solution)/shard_map/all_to_all | solution.py:224
  160.1 0.1 shard_map.89
  160.2 0.6 copy.9
  (9 shorter events, 0.0 us)
Async XLA Ops:
  0.0 0.8 copy-start.4
  0.8 0.7 copy-start.5
  1.4 0.7 copy-start.7
  45.4 1.2 copy-start.3
  47.0 1.4 copy-start
  48.4 7.2 %copy-start.1 = (bf16[1,2048,224]{1,2,0:T(8,128)(2,1)S(1)}, bf16[1,2048,224]{1,2,0:T(8,128)(2,1)}, u32[]{:S(2)}) copy-start(bf16[1,2048,224]{1,2,0:T(8,128)(2,1)} %param.12) | copy-start | bytes 2752516
  48.4 39.7 %all-to-all-start.1 = ((bf16[16,552,128]{2,1,0:T(8,128)(2,1)}), bf16[16,552,128]{2,1,0:T(8,128)(2,1)S(1)}, u32[]{:S(2)}, u32[]{:S(2)}) async-start(bf16[16,552,128]{2,1,0:T(8,128)(2,1)} %copy-done), calls=%async_computation.1 | async-start | bytes 4521984 | tf_op jit(solution)/shard_map/all_to_all | solution.py:201
  55.6 34.6 %collective-permute-start = (bf16[224,2048]{1,0:T(8,128)(2,1)S(1)}, bf16[224,2048]{1,0:T(8,128)(2,1)}, u32[]{:S(2)}, u32[]{:S(2)}) collective-permute-start(bf16[224,2048]{1,0:T(8,128)(2,1)S(1)} %bitcast.11), channel_id=1, source_target_pairs={{0,16},{16,0},{1,17},{17,1},{2,18},{18,2},{3,19},{19,3},{4,20},{20... | collective-permute-start | bytes 2752520 | tf_op jit(solution)/shard_map/ppermute | solution.py:191
  57.5 32.7 %collective-permute-start.1 = (bf16[224,2048]{1,0:T(8,128)(2,1)}, bf16[224,2048]{1,0:T(8,128)(2,1)}, u32[]{:S(2)}, u32[]{:S(2)}) collective-permute-start(bf16[224,2048]{1,0:T(8,128)(2,1)} %bitcast.13), channel_id=1, source_target_pairs={{0,16},{16,0},{1,17},{17,1},{2,18},{18,2},{3,19},{19,3},{4,20},{20... | collective-permute-start | bytes 2752520 | tf_op jit(solution)/shard_map/ppermute | solution.py:192
  88.1 2.1 %copy-start.2 = (bf16[1,2048,224]{1,2,0:T(8,128)(2,1)S(1)}, bf16[1,2048,224]{1,2,0:T(8,128)(2,1)}, u32[]{:S(2)}) copy-start(bf16[1,2048,224]{1,2,0:T(8,128)(2,1)} %param.13) | copy-start | bytes 2752516
  88.1 4.5 %collective-permute-start.2 = (bf16[16,224,128]{2,1,0:T(8,128)(2,1)S(1)}, bf16[16,224,128]{2,1,0:T(8,128)(2,1)S(1)}, u32[]{:S(2)}, u32[]{:S(2)}) collective-permute-start(bf16[16,224,128]{2,1,0:T(8,128)(2,1)S(1)} %slice.4), channel_id=1, source_target_pairs={{0,16},{16,0},{1,17},{17,1},{2,18},{18,2},{3,19},{19,3},{4,20},{20... | collective-permute-start | bytes 2752520 | tf_op jit(solution)/shard_map/ppermute | solution.py:202
  94.1 46.8 %copy-start.6 = (f32[128,2]{0,1:T(2,128)S(1)}, f32[128,2]{0,1:T(2,128)}, u32[]{:S(2)}) copy-start(f32[128,2]{0,1:T(2,128)} %param.11) | copy-start | bytes 3076
  94.2 65.9 %copy-start.8 = (f32[128]{0:T(128)S(1)}, f32[128]{0:T(128)}, u32[]{:S(2)}) copy-start(f32[128]{0:T(128)} %param.15) | copy-start | bytes 1540
  118.5 30.4 %all-to-all-start.3 = ((bf16[32,2,640]{2,1,0:T(2,128)(2,1)}), bf16[32,2,640]{2,1,0:T(2,128)(2,1)S(1)}, u32[]{:S(2)}, u32[]{:S(2)}) async-start(bf16[32,2,640]{2,1,0:T(2,128)(2,1)} %shard_map.86), calls=%async_computation.3 | async-start | bytes 163840 | tf_op jit(solution)/shard_map/all_to_all | solution.py:52

commit v6 on v3

--- a/solution.py
+++ b/solution.py
@@ -15,6 +15,7 @@
 W = D // TP
 HID = 224
 EXTRA = 8
+FIRST = 16
 FRONT = ROWS + EXTRA
 EPS = 1e-05
 
@@ -23,29 +24,51 @@
 MIB = 1 << 20
 
 
-def call(kernel, outs, mib, free=0, **kw):
+def call(kernel, outs, mib, hbm=0, **kw):
     def run(*operands):
-        near = operands[: len(operands) - free]
-        far = operands[len(operands) - free :]
         many = isinstance(outs, list)
+        near = len(operands) - hbm
         vmem = pl.BlockSpec(memory_space=pltpu.VMEM)
+        spaces = [pltpu.VMEM] * near + [pltpu.HBM] * hbm
         return pl.pallas_call(
             kernel,
             out_shape=[pltpu.VMEM(s, d) for s, d in outs] if many else pltpu.VMEM(*outs),
-            in_specs=[vmem] * len(near) + [pl.BlockSpec(memory_space=pl.ANY)] * free,
+            in_specs=[pl.BlockSpec(memory_space=space) for space in spaces],
             out_specs=[vmem] * len(outs) if many else vmem,
             compiler_params=pltpu.CompilerParams(vmem_limit_bytes=mib * MIB),
             **kw,
-        )(*[pltpu.with_memory_space_constraint(x, pltpu.VMEM) for x in near], *far)
+        )(
+            *[
+                pltpu.with_memory_space_constraint(x, space)
+                for x, space in zip(operands, spaces)
+            ]
+        )
 
     return run
 
 
 def place_of(slot, expert):
-    return (slot // 2) * (2 * EXPERTS) + 2 * expert + slot % 2
-
-
-def dispatch_kernel(routing_ref, tokens_ref, gain_ref, out_ref, place_ref, gain_out_ref):
+    position = (expert + EXPERTS - FIRST) % EXPERTS
+    return (slot // 2) * (2 * EXPERTS) + 2 * position + slot % 2
+
+
+def exchange(blocks):
+    order = [(p + FIRST) % EXPERTS for p in range(EXPERTS)]
+    return lax.all_to_all(blocks, "z", 0, 0, axis_index_groups=[order], tiled=True)
+
+
+def dispatch_kernel(
+    routing_far, tokens_far, gain_far, out_ref, place_ref, gain_out_ref,
+    routing_ref, tokens_ref, gain_ref, sems,
+):
+    copies = [
+        pltpu.make_async_copy(routing_far, routing_ref, sems.at[0]),
+        pltpu.make_async_copy(tokens_far, tokens_ref, sems.at[1]),
+        pltpu.make_async_copy(gain_far, gain_ref, sems.at[2]),
+    ]
+    for copy in copies:
+        copy.start()
+    copies[0].wait()
     expert0, expert1 = routing_ref[0:1], routing_ref[1:2]
     index = lax.broadcasted_iota(jnp.int32, (EXPERTS, TOK), 0)
     hit0, hit1 = index == expert0, index == expert1
@@ -64,10 +87,12 @@
     place_ref[1:2] = place1
     spots = lax.broadcasted_iota(jnp.int32, (ROWS, TOK), 0)
     picker = jnp.where((spots == place0) | (spots == place1), 1.0, 0.0).astype(BF16)
+    copies[1].wait()
     rows = jnp.dot(picker, tokens_ref[...], preferred_element_type=F32).astype(BF16)
     for block in range(CAP // 2):
         piece = rows[block * 64 : (block + 1) * 64]
         out_ref[:, :, block * W : (block + 1) * W] = piece.reshape(EXPERTS, 2, W)
+    copies[2].wait()
     gain = gain_ref[...]
     high = gain.astype(BF16).astype(F32)
     mid = (gain - high).astype(BF16).astype(F32)
@@ -77,8 +102,7 @@
     gain_out_ref[...] = parts.astype(BF16)
 
 
-def prepare_kernel(place_ref, weight_ref, gate_ref, up_ref, pick_ref, weight_out_ref):
-    del gate_ref, up_ref
+def prepare_kernel(place_ref, weight_ref, pick_ref, weight_out_ref):
     spots = lax.broadcasted_iota(jnp.int32, (TOK, ROWS), 1).astype(F32)
     for k in range(2):
         place = jnp.broadcast_to(place_ref[k : k + 1].astype(F32), (TOK, TOK)).T
@@ -86,7 +110,9 @@
         weight_out_ref[k] = jnp.broadcast_to(weight_ref[k : k + 1], (TOK, TOK)).T
 
 
-def spread_kernel(rows_ref, gain_ref, down_ref, out_ref):
+def spread_kernel(rows_ref, gain_ref, down_far, out_ref, sem):
+    down = pltpu.make_async_copy(down_far, out_ref.at[:, FRONT:], sem)
+    down.start()
     gain = gain_ref[...]
     for block in range(CAP // 2):
         piece = rows_ref[:, :, block * W : (block + 1) * W].reshape(64, W)
@@ -94,7 +120,7 @@
             out_ref[peer, block * 64 : (block + 1) * 64] = piece
     for peer in range(TP):
         out_ref[peer, ROWS:FRONT] = gain
-        out_ref[peer, FRONT:] = down_ref[peer]
+    down.wait()
 
 
 def hidden_kernel(x_ref, gate_a, gate_b, up_a, up_b, out_ref, normed_ref):
@@ -117,10 +143,13 @@
 
 def output_kernel(hidden_ref, x_ref, down_ref, out_ref):
     first, second = hidden_ref[0], hidden_ref[1]
-    for t in range(TP):
-        part = jnp.dot(first, x_ref[t, FRONT:], preferred_element_type=F32)
-        part = part + jnp.dot(second, down_ref[t], preferred_element_type=F32)
-        out_ref[t] = part.astype(BF16)
+    for t in range(0, TP, 2):
+        own = jnp.concatenate([x_ref[t, FRONT:], x_ref[t + 1, FRONT:]], axis=1)
+        other = jnp.concatenate([down_ref[t], down_ref[t + 1]], axis=1)
+        part = jnp.dot(first, own, preferred_element_type=F32)
+        part = (part + jnp.dot(second, other, preferred_element_type=F32)).astype(BF16)
+        out_ref[t] = part[:, :W]
+        out_ref[t + 1] = part[:, W:]
 
 
 def reduce_kernel(parts_ref, out_ref):
@@ -166,17 +195,29 @@
         dispatch_kernel,
         [((EXPERTS, 2, 640), BF16), ((2, TOK), jnp.int32), ((EXTRA, W), BF16)],
         4,
+        hbm=3,
+        scratch_shapes=[
+            pltpu.VMEM((2, TOK), jnp.int32),
+            pltpu.VMEM((TOK, W), BF16),
+            pltpu.VMEM((1, W), F32),
+            pltpu.SemaphoreType.DMA((3,)),
+        ],
     )(routing.T, tokens, norm_gain.reshape(1, W))
-    arrived = lax.all_to_all(outgoing, "z", 0, 0, tiled=True)
+    arrived = exchange(outgoing)
     gate_other = lax.ppermute(gate_own, "c", swap)
     up_other = lax.ppermute(up_own, "c", swap)
     pick, weight = call(
         prepare_kernel,
         [((2, TOK, ROWS), BF16), ((2, TOK, W), F32)],
         4,
-        free=2,
-    )(place, route_weight.T, gate_other, up_other)
-    spread = call(spread_kernel, ((TP, FRONT + HID, W), BF16), 4)(
+    )(place, route_weight.T)
+    spread = call(
+        spread_kernel,
+        ((TP, FRONT + HID, W), BF16),
+        4,
+        hbm=1,
+        scratch_shapes=[pltpu.SemaphoreType.DMA],
+    )(
         arrived, gain_parts, down_weight.reshape(TP, HID, W)
     )
     features = lax.all_to_all(spread, "t", 0, 0, tiled=True)
@@ -192,7 +233,7 @@
     )
     parts = lax.all_to_all(parts, "t", 0, 0, tiled=True)
     reduced = call(reduce_kernel, ((EXPERTS, 2, 640), BF16), 4)(parts)
-    returned = lax.all_to_all(reduced, "z", 0, 0, tiled=True)
+    returned = exchange(reduced)
     mixed, square = call(
         combine_kernel, [((TOK, W), F32), ((TP, 1, TOK), F32)], 4
     )(returned, pick, weight)

time: 174 us -> 160 us (0.920)
  the two profiles are of different devices: /device:TPU:2 before, /device:TPU:32 now
where the time goes in v6:
time: 160 us; the launch traced here: 159 us
  blocking collectives  77.3 us (48%)
  starting transfers between devices  36 us (22%)
  waiting for transfers between devices  35.9 us (22%)
  Pallas kernels  7.86 us (5%)
  local copies, waits for them, and re-layouts  2.08 us (1%)
    all_to_all x1, blocking collectives, exchange(): lax.all_to_all(blocks, 'z', 0, 0, axis_index_groups=[order], tiled=True)  43 us
    all_to_all x1, waiting for transfers between devices, shards(): features = lax.all_to_all(spread, 't', 0, 0, tiled=True)  28.2 us
    all_to_all x1, blocking collectives, shards(): parts = lax.all_to_all(parts, 't', 0, 0, tiled=True)  23.6 us
    all_to_all x1, starting transfers between devices, exchange(): lax.all_to_all(blocks, 'z', 0, 0, axis_index_groups=[order], tiled=True)  22.4 us
    all_to_all x1, blocking collectives, shards(): squares = lax.all_to_all(square, 't', 0, 0, tiled=True)  10.8 us
    pallas_call x8, Pallas kernels, run(): pl.pallas_call(kernel, out_shape=[pltpu.VMEM(s, d) for s, d in outs] if m...  7.86 us
    all_to_all x1, waiting for transfers between devices, exchange(): lax.all_to_all(blocks, 'z', 0, 0, axis_index_groups=[order], tiled=True)  7.79 us
    all_to_all x1, starting transfers between devices, shards(): features = lax.all_to_all(spread, 't', 0, 0, tiled=True)  7.17 us
  transfers between devices with their start and end apart: 5, of which 2 were waited for; matrix products, arithmetic and copies ran while one was open for 0% of the time, Pallas kernels for 2%

profile of v6, /device:TPU:32, one launch (start us, length us, event | category | flops | bytes accessed | tf_op | source)
XLA Modules:
  0.0 159.3 jit_solution(5000143499782752857)
XLA Ops:
  0.0 1.1 shard_map.82
  1.1 43.0 %all_to_all.25.rows_ref = bf16[32,2,640]{2,1,0:T(2,128)(2,1)S(1)} all-to-all(bf16[32,2,640]{2,1,0:T(2,128)(2,1)S(1)} %get-tuple-element.12), channel_id=1, replica_groups={{512,544,576,608,640,672,704,736,768,800,832,864,896,928,960,992,0,32,6..., dimensions={0} | all-to-all | bytes 163840 | tf_op jit(solution)/shard_map/all_to_all | solution.py:57
  44.1 1.2 shard_map.83
  45.3 0.0 copy-start
  45.3 1.4 copy-done
  46.7 0.0 copy-start.1
  46.7 7.2 %all-to-all-start.1 = ((bf16[16,552,128]{2,1,0:T(8,128)(2,1)}), bf16[16,552,128]{2,1,0:T(8,128)(2,1)S(1)}, u32[]{:S(2)}, u32[]{:S(2)}) async-start(bf16[16,552,128]{2,1,0:T(8,128)(2,1)} %copy-done), calls=%async_computation.1 | async-start | bytes 4521984 | tf_op jit(solution)/shard_map/all_to_all | solution.py:223
  53.9 0.0 copy-done.1
  53.9 1.9 %collective-permute-start = (bf16[224,2048]{1,0:T(8,128)(2,1)S(1)}, bf16[224,2048]{1,0:T(8,128)(2,1)}, u32[]{:S(2)}, u32[]{:S(2)}) collective-permute-start(bf16[224,2048]{1,0:T(8,128)(2,1)S(1)} %bitcast.11), channel_id=1, source_target_pairs={{0,16},{16,0},{1,17},{17,1},{2,18},{18,2},{3,19},{19,3},{4,20},{20... | collective-permute-start | bytes 2752520 | tf_op jit(solution)/shard_map/ppermute | solution.py:207
  55.8 2.4 %collective-permute-start.1 = (bf16[224,2048]{1,0:T(8,128)(2,1)}, bf16[224,2048]{1,0:T(8,128)(2,1)}, u32[]{:S(2)}, u32[]{:S(2)}) collective-permute-start(bf16[224,2048]{1,0:T(8,128)(2,1)} %bitcast.13), channel_id=1, source_target_pairs={{0,16},{16,0},{1,17},{17,1},{2,18},{18,2},{3,19},{19,3},{4,20},{20... | collective-permute-start | bytes 2752520 | tf_op jit(solution)/shard_map/ppermute | solution.py:208
  58.2 28.2 %all-to-all-done.1.x_ref = bf16[16,552,128]{2,1,0:T(8,128)(2,1)S(1)} async-done(((bf16[16,552,128]{2,1,0:T(8,128)(2,1)}), bf16[16,552,128]{2,1,0:T(8,128)(2,1)S(1)}, u32[]{:S(2)}, u32[]{:S(2)}) %all-to-all-start.1) | async-done | bytes 2261024 | tf_op jit(solution)/shard_map/all_to_all | solution.py:223
  86.4 0.1 slice.4
  86.4 2.1 %collective-permute-start.2 = (bf16[16,224,128]{2,1,0:T(8,128)(2,1)S(1)}, bf16[16,224,128]{2,1,0:T(8,128)(2,1)S(1)}, u32[]{:S(2)}, u32[]{:S(2)}) collective-permute-start(bf16[16,224,128]{2,1,0:T(8,128)(2,1)S(1)} %slice.4), channel_id=1, source_target_pairs={{0,16},{16,0},{1,17},{17,1},{2,18},{18,2},{3,19},{19,3},{4,20},{20... | collective-permute-start | bytes 2752520 | tf_op jit(solution)/shard_map/ppermute | solution.py:224
  88.5 0.0 collective-permute-done.gate_b
  88.5 0.0 collective-permute-done.1.up_b
  88.5 0.0 copy-done.2
  88.5 3.2 %shard_map.84.hidden_ref = bf16[2,320,224]{2,1,0:T(8,128)(2,1)S(1)} custom-call(bf16[16,552,128]{2,1,0:T(8,128)(2,1)S(1)} %all-to-all-done.1.x_ref, bf16[224,2048]{1,0:T(8,128)(2,1)S(1)} %bitcast.12, bf16[224,2048]{1,0:T(8,128)(2,1)} %collective-permute-done.gate_b, bf16[224,2048]{1,0:T(8,128)(2,1)S(1)} %bitcast.14, ...), custom_call_target="tpu_custom_call" | custom-call | tf_op jit(solution)/shard_map/pallas_call | solution.py:33
  91.8 0.0 collective-permute-done.2.down_ref
  91.8 0.8 shard_map.85
  92.6 0.0 copy-start.3
  92.7 0.0 copy-start.4
  92.7 23.6 %all_to_all.26.parts_ref = bf16[16,320,128]{2,1,0:T(8,128)(2,1)S(1)} all-to-all(bf16[16,320,128]{2,1,0:T(8,128)(2,1)S(1)} %shard_map.85), channel_id=1, replica_groups=mesh['z'=32,'c'=2,'t'=16] {'t'}, dimensions={0} | all-to-all | bytes 2621440 | tf_op jit(solution)/shard_map/all_to_all | solution.py:234
  116.2 0.8 shard_map.86
  117.1 22.4 %all-to-all-start.3 = ((bf16[32,2,640]{2,1,0:T(2,128)(2,1)}), bf16[32,2,640]{2,1,0:T(2,128)(2,1)S(1)}, u32[]{:S(2)}, u32[]{:S(2)}) async-start(bf16[32,2,640]{2,1,0:T(2,128)(2,1)} %shard_map.86), calls=%async_computation.3 | async-start | bytes 163840 | tf_op jit(solution)/shard_map/all_to_all | solution.py:57
  139.5 0.0 copy-done.3
  139.5 0.2 shard_map.87
  139.7 7.8 %all-to-all-done.3.rows_ref = bf16[32,2,640]{2,1,0:T(2,128)(2,1)S(1)} async-done(((bf16[32,2,640]{2,1,0:T(2,128)(2,1)}), bf16[32,2,640]{2,1,0:T(2,128)(2,1)S(1)}, u32[]{:S(2)}, u32[]{:S(2)}) %all-to-all-start.3) | async-done | bytes 81952 | tf_op jit(solution)/shard_map/all_to_all | solution.py:57
  147.5 0.3 shard_map.88
  147.8 10.8 %all_to_all.27.square_ref = f32[16,1,128]{2,1,0:T(1,128)S(1)} all-to-all(f32[16,1,128]{2,1,0:T(1,128)S(1)} %get-tuple-element.18), channel_id=1, replica_groups=mesh['z'=32,'c'=2,'t'=16] {'t'}, dimensions={0} | all-to-all | bytes 16384 | tf_op jit(solution)/shard_map/all_to_all | solution.py:240
  158.6 0.0 copy-done.4
  158.6 0.1 shard_map.89
  158.7 0.6 copy.9
  (1 shorter events, 0.0 us)
Async XLA Ops:
  45.3 1.4 copy-start
  46.7 7.2 %copy-start.1 = (bf16[1,2048,224]{1,2,0:T(8,128)(2,1)S(1)}, bf16[1,2048,224]{1,2,0:T(8,128)(2,1)}, u32[]{:S(2)}) copy-start(bf16[1,2048,224]{1,2,0:T(8,128)(2,1)} %param.12) | copy-start | bytes 2752516
  46.7 39.7 %all-to-all-start.1 = ((bf16[16,552,128]{2,1,0:T(8,128)(2,1)}), bf16[16,552,128]{2,1,0:T(8,128)(2,1)S(1)}, u32[]{:S(2)}, u32[]{:S(2)}) async-start(bf16[16,552,128]{2,1,0:T(8,128)(2,1)} %copy-done), calls=%async_computation.1 | async-start | bytes 4521984 | tf_op jit(solution)/shard_map/all_to_all | solution.py:223
  53.9 34.6 %collective-permute-start = (bf16[224,2048]{1,0:T(8,128)(2,1)S(1)}, bf16[224,2048]{1,0:T(8,128)(2,1)}, u32[]{:S(2)}, u32[]{:S(2)}) collective-permute-start(bf16[224,2048]{1,0:T(8,128)(2,1)S(1)} %bitcast.11), channel_id=1, source_target_pairs={{0,16},{16,0},{1,17},{17,1},{2,18},{18,2},{3,19},{19,3},{4,20},{20... | collective-permute-start | bytes 2752520 | tf_op jit(solution)/shard_map/ppermute | solution.py:207
  55.8 32.7 %collective-permute-start.1 = (bf16[224,2048]{1,0:T(8,128)(2,1)}, bf16[224,2048]{1,0:T(8,128)(2,1)}, u32[]{:S(2)}, u32[]{:S(2)}) collective-permute-start(bf16[224,2048]{1,0:T(8,128)(2,1)} %bitcast.13), channel_id=1, source_target_pairs={{0,16},{16,0},{1,17},{17,1},{2,18},{18,2},{3,19},{19,3},{4,20},{20... | collective-permute-start | bytes 2752520 | tf_op jit(solution)/shard_map/ppermute | solution.py:208
  86.4 2.1 %copy-start.2 = (bf16[1,2048,224]{1,2,0:T(8,128)(2,1)S(1)}, bf16[1,2048,224]{1,2,0:T(8,128)(2,1)}, u32[]{:S(2)}) copy-start(bf16[1,2048,224]{1,2,0:T(8,128)(2,1)} %param.13) | copy-start | bytes 2752516
  86.4 5.3 %collective-permute-start.2 = (bf16[16,224,128]{2,1,0:T(8,128)(2,1)S(1)}, bf16[16,224,128]{2,1,0:T(8,128)(2,1)S(1)}, u32[]{:S(2)}, u32[]{:S(2)}) collective-permute-start(bf16[16,224,128]{2,1,0:T(8,128)(2,1)S(1)} %slice.4), channel_id=1, source_target_pairs={{0,16},{16,0},{1,17},{17,1},{2,18},{18,2},{3,19},{19,3},{4,20},{20... | collective-permute-start | bytes 2752520 | tf_op jit(solution)/shard_map/ppermute | solution.py:224
  92.6 46.8 %copy-start.3 = (f32[128,2]{0,1:T(2,128)S(1)}, f32[128,2]{0,1:T(2,128)}, u32[]{:S(2)}) copy-start(f32[128,2]{0,1:T(2,128)} %param.11) | copy-start | bytes 3076
  92.7 65.9 %copy-start.4 = (f32[128]{0:T(128)S(1)}, f32[128]{0:T(128)}, u32[]{:S(2)}) copy-start(f32[128]{0:T(128)} %param.15) | copy-start | bytes 1540
  117.1 30.5 %all-to-all-start.3 = ((bf16[32,2,640]{2,1,0:T(2,128)(2,1)}), bf16[32,2,640]{2,1,0:T(2,128)(2,1)S(1)}, u32[]{:S(2)}, u32[]{:S(2)}) async-start(bf16[32,2,640]{2,1,0:T(2,128)(2,1)} %shard_map.86), calls=%async_computation.3 | async-start | bytes 163840 | tf_op jit(solution)/shard_map/all_to_all | solution.py:57

commit v7 on v6

--- a/solution.py
+++ b/solution.py
@@ -16,6 +16,7 @@
 HID = 224
 EXTRA = 8
 FIRST = 16
+FIRST_TP = 10
 FRONT = ROWS + EXTRA
 EPS = 1e-05
 
@@ -55,6 +56,11 @@
 def exchange(blocks):
     order = [(p + FIRST) % EXPERTS for p in range(EXPERTS)]
     return lax.all_to_all(blocks, "z", 0, 0, axis_index_groups=[order], tiled=True)
+
+
+def across_plane(blocks):
+    order = [p ^ FIRST_TP for p in range(TP)]
+    return lax.all_to_all(blocks, "t", 0, 0, axis_index_groups=[order], tiled=True)
 
 
 def dispatch_kernel(
@@ -110,9 +116,15 @@
         weight_out_ref[k] = jnp.broadcast_to(weight_ref[k : k + 1], (TOK, TOK)).T
 
 
-def spread_kernel(rows_ref, gain_ref, down_far, out_ref, sem):
-    down = pltpu.make_async_copy(down_far, out_ref.at[:, FRONT:], sem)
-    down.start()
+def spread_kernel(rows_ref, gain_ref, down_far, out_ref, sems):
+    copies = [
+        pltpu.make_async_copy(
+            down_far.at[peer ^ FIRST_TP], out_ref.at[peer, FRONT:], sems.at[peer]
+        )
+        for peer in range(TP)
+    ]
+    for copy in copies:
+        copy.start()
     gain = gain_ref[...]
     for block in range(CAP // 2):
         piece = rows_ref[:, :, block * W : (block + 1) * W].reshape(64, W)
@@ -120,7 +132,8 @@
             out_ref[peer, block * 64 : (block + 1) * 64] = piece
     for peer in range(TP):
         out_ref[peer, ROWS:FRONT] = gain
-    down.wait()
+    for copy in copies:
+        copy.wait()
 
 
 def hidden_kernel(x_ref, gate_a, gate_b, up_a, up_b, out_ref, normed_ref):
@@ -129,9 +142,10 @@
         piece = x_ref[t, :ROWS].astype(F32)
         total = total + piece * piece
     scale = lax.rsqrt(jnp.sum(total, axis=1, keepdims=True) / D + EPS)
-    for t in range(TP):
-        gain = jnp.sum(x_ref[t, ROWS:FRONT].astype(F32), axis=0, keepdims=True)
-        piece = x_ref[t, :ROWS].astype(F32)
+    for p in range(TP):
+        gain = jnp.sum(x_ref[p, ROWS:FRONT].astype(F32), axis=0, keepdims=True)
+        piece = x_ref[p, :ROWS].astype(F32)
+        t = p ^ FIRST_TP
         normed_ref[:, t * W : (t + 1) * W] = (piece * scale * gain).astype(BF16)
     normed = normed_ref[...]
     across = (((1,), (1,)), ((), ()))
@@ -216,11 +230,11 @@
         ((TP, FRONT + HID, W), BF16),
         4,
         hbm=1,
-        scratch_shapes=[pltpu.SemaphoreType.DMA],
+        scratch_shapes=[pltpu.SemaphoreType.DMA((TP,))],
     )(
         arrived, gain_parts, down_weight.reshape(TP, HID, W)
     )
-    features = lax.all_to_all(spread, "t", 0, 0, tiled=True)
+    features = across_plane(spread)
     down_other = lax.ppermute(features[:, FRONT:], "c", swap)
     hidden = call(
         hidden_kernel,
@@ -231,13 +245,13 @@
     parts = call(output_kernel, ((TP, ROWS, W), BF16), 8)(
         hidden, features, down_other
     )
-    parts = lax.all_to_all(parts, "t", 0, 0, tiled=True)
+    parts = across_plane(parts)
     reduced = call(reduce_kernel, ((EXPERTS, 2, 640), BF16), 4)(parts)
     returned = exchange(reduced)
     mixed, square = call(
         combine_kernel, [((TOK, W), F32), ((TP, 1, TOK), F32)], 4
     )(returned, pick, weight)
-    squares = lax.all_to_all(square, "t", 0, 0, tiled=True)
+    squares = across_plane(square)
     return call(finish_kernel, ((TOK, W), BF16), 4)(mixed, squares, final_gain.reshape(1, W))
 
 

time: 160 us -> 157 us (0.981)
  the two profiles are of different devices: /device:TPU:32 before, /device:TPU:2 now
where the time goes in v7:
time: 157 us; the launch traced here: 156 us
  blocking collectives  78.9 us (50%)
  starting transfers between devices  37.5 us (24%)
  waiting for transfers between devices  29.7 us (19%)
  Pallas kernels  8 us (5%)
  local copies, waits for them, and re-layouts  2.08 us (1%)
    all_to_all x1, blocking collectives, exchange(): lax.all_to_all(blocks, 'z', 0, 0, axis_index_groups=[order], tiled=True)  43.4 us
    all_to_all x2, blocking collectives, across_plane(): lax.all_to_all(blocks, 't', 0, 0, axis_index_groups=[order], tiled=True)  35.5 us
    all_to_all x1, starting transfers between devices, exchange(): lax.all_to_all(blocks, 'z', 0, 0, axis_index_groups=[order], tiled=True)  23.3 us
    all_to_all x1, waiting for transfers between devices, across_plane(): lax.all_to_all(blocks, 't', 0, 0, axis_index_groups=[order], tiled=True)  23 us
    pallas_call x8, Pallas kernels, run(): pl.pallas_call(kernel, out_shape=[pltpu.VMEM(s, d) for s, d in outs] if m...  8 us
    all_to_all x1, starting transfers between devices, across_plane(): lax.all_to_all(blocks, 't', 0, 0, axis_index_groups=[order], tiled=True)  7.83 us
    all_to_all x1, waiting for transfers between devices, exchange(): lax.all_to_all(blocks, 'z', 0, 0, axis_index_groups=[order], tiled=True)  6.72 us
  transfers between devices with their start and end apart: 5, of which 2 were waited for; matrix products, arithmetic and copies ran while one was open for 0% of the time, Pallas kernels for 2%

profile of v7, /device:TPU:2, one launch (start us, length us, event | category | flops | bytes accessed | tf_op | source)
XLA Modules:
  0.0 156.3 jit_solution(4223711233644673162)
XLA Ops:
  0.0 1.1 shard_map.82
  1.1 43.4 %all_to_all.25.rows_ref = bf16[32,2,640]{2,1,0:T(2,128)(2,1)S(1)} all-to-all(bf16[32,2,640]{2,1,0:T(2,128)(2,1)S(1)} %get-tuple-element.12), channel_id=1, replica_groups={{512,544,576,608,640,672,704,736,768,800,832,864,896,928,960,992,0,32,6..., dimensions={0} | all-to-all | bytes 163840 | tf_op jit(solution)/shard_map/all_to_all | solution.py:58
  44.5 1.3 shard_map.83
  45.9 0.0 copy-start
  45.9 1.4 copy-done
  47.2 0.0 copy-start.1
  47.2 7.8 %all-to-all-start.1 = ((bf16[16,552,128]{2,1,0:T(8,128)(2,1)}), bf16[16,552,128]{2,1,0:T(8,128)(2,1)S(1)}, u32[]{:S(2)}, u32[]{:S(2)}) async-start(bf16[16,552,128]{2,1,0:T(8,128)(2,1)} %copy-done), calls=%async_computation.1 | async-start | bytes 4521984 | tf_op jit(solution)/shard_map/all_to_all | solution.py:63
  55.1 0.0 copy-done.1
  55.1 1.9 %collective-permute-start = (bf16[224,2048]{1,0:T(8,128)(2,1)S(1)}, bf16[224,2048]{1,0:T(8,128)(2,1)}, u32[]{:S(2)}, u32[]{:S(2)}) collective-permute-start(bf16[224,2048]{1,0:T(8,128)(2,1)S(1)} %bitcast.11), channel_id=1, source_target_pairs={{0,16},{16,0},{1,17},{17,1},{2,18},{18,2},{3,19},{19,3},{4,20},{20... | collective-permute-start | bytes 2752520 | tf_op jit(solution)/shard_map/ppermute | solution.py:221
  57.0 2.4 %collective-permute-start.1 = (bf16[224,2048]{1,0:T(8,128)(2,1)}, bf16[224,2048]{1,0:T(8,128)(2,1)}, u32[]{:S(2)}, u32[]{:S(2)}) collective-permute-start(bf16[224,2048]{1,0:T(8,128)(2,1)} %bitcast.13), channel_id=1, source_target_pairs={{0,16},{16,0},{1,17},{17,1},{2,18},{18,2},{3,19},{19,3},{4,20},{20... | collective-permute-start | bytes 2752520 | tf_op jit(solution)/shard_map/ppermute | solution.py:222
  59.4 23.0 %all-to-all-done.1.x_ref = bf16[16,552,128]{2,1,0:T(8,128)(2,1)S(1)} async-done(((bf16[16,552,128]{2,1,0:T(8,128)(2,1)}), bf16[16,552,128]{2,1,0:T(8,128)(2,1)S(1)}, u32[]{:S(2)}, u32[]{:S(2)}) %all-to-all-start.1) | async-done | bytes 2261024 | tf_op jit(solution)/shard_map/all_to_all | solution.py:63
  82.4 0.1 slice.4
  82.5 2.1 %collective-permute-start.2 = (bf16[16,224,128]{2,1,0:T(8,128)(2,1)S(1)}, bf16[16,224,128]{2,1,0:T(8,128)(2,1)S(1)}, u32[]{:S(2)}, u32[]{:S(2)}) collective-permute-start(bf16[16,224,128]{2,1,0:T(8,128)(2,1)S(1)} %slice.4), channel_id=1, source_target_pairs={{0,16},{16,0},{1,17},{17,1},{2,18},{18,2},{3,19},{19,3},{4,20},{20... | collective-permute-start | bytes 2752520 | tf_op jit(solution)/shard_map/ppermute | solution.py:238
  84.5 0.0 collective-permute-done.gate_b
  84.5 0.0 collective-permute-done.1.up_b
  84.5 0.0 copy-done.2
  84.6 3.2 %shard_map.84.hidden_ref = bf16[2,320,224]{2,1,0:T(8,128)(2,1)S(1)} custom-call(bf16[16,552,128]{2,1,0:T(8,128)(2,1)S(1)} %all-to-all-done.1.x_ref, bf16[224,2048]{1,0:T(8,128)(2,1)S(1)} %bitcast.12, bf16[224,2048]{1,0:T(8,128)(2,1)} %collective-permute-done.gate_b, bf16[224,2048]{1,0:T(8,128)(2,1)S(1)} %bitcast.14, ...), custom_call_target="tpu_custom_call" | custom-call | tf_op jit(solution)/shard_map/pallas_call | solution.py:34
  87.8 0.0 collective-permute-done.2.down_ref
  87.8 0.8 shard_map.85
  88.7 0.0 copy-start.3
  88.7 0.0 copy-start.4
  88.7 24.4 %all_to_all.26.parts_ref = bf16[16,320,128]{2,1,0:T(8,128)(2,1)S(1)} all-to-all(bf16[16,320,128]{2,1,0:T(8,128)(2,1)S(1)} %shard_map.85), channel_id=1, replica_groups={{10,11,8,9,14,15,12,13,2,3,0,1,6,7,4,5},{26,27,24,25,30,31,28,29,18,19,..., dimensions={0} | all-to-all | bytes 2621440 | tf_op jit(solution)/shard_map/all_to_all | solution.py:63
  113.1 0.8 shard_map.86
  114.0 23.3 %all-to-all-start.3 = ((bf16[32,2,640]{2,1,0:T(2,128)(2,1)}), bf16[32,2,640]{2,1,0:T(2,128)(2,1)S(1)}, u32[]{:S(2)}, u32[]{:S(2)}) async-start(bf16[32,2,640]{2,1,0:T(2,128)(2,1)} %shard_map.86), calls=%async_computation.3 | async-start | bytes 163840 | tf_op jit(solution)/shard_map/all_to_all | solution.py:58
  137.3 0.0 copy-done.3
  137.3 0.2 shard_map.87
  137.5 6.7 %all-to-all-done.3.rows_ref = bf16[32,2,640]{2,1,0:T(2,128)(2,1)S(1)} async-done(((bf16[32,2,640]{2,1,0:T(2,128)(2,1)}), bf16[32,2,640]{2,1,0:T(2,128)(2,1)S(1)}, u32[]{:S(2)}, u32[]{:S(2)}) %all-to-all-start.3) | async-done | bytes 81952 | tf_op jit(solution)/shard_map/all_to_all | solution.py:58
  144.3 0.3 shard_map.88
  144.6 11.0 %all_to_all.27.square_ref = f32[16,1,128]{2,1,0:T(1,128)S(1)} all-to-all(f32[16,1,128]{2,1,0:T(1,128)S(1)} %get-tuple-element.18), channel_id=1, replica_groups={{10,11,8,9,14,15,12,13,2,3,0,1,6,7,4,5},{26,27,24,25,30,31,28,29,18,19,..., dimensions={0} | all-to-all | bytes 16384 | tf_op jit(solution)/shard_map/all_to_all | solution.py:63
  155.6 0.0 copy-done.4
  155.6 0.1 shard_map.89
  155.7 0.6 copy.9
  (1 shorter events, 0.0 us)
Async XLA Ops:
  45.9 1.4 copy-start
  47.2 7.8 %copy-start.1 = (bf16[1,2048,224]{1,2,0:T(8,128)(2,1)S(1)}, bf16[1,2048,224]{1,2,0:T(8,128)(2,1)}, u32[]{:S(2)}) copy-start(bf16[1,2048,224]{1,2,0:T(8,128)(2,1)} %param.12) | copy-start | bytes 2752516
  47.2 35.1 %all-to-all-start.1 = ((bf16[16,552,128]{2,1,0:T(8,128)(2,1)}), bf16[16,552,128]{2,1,0:T(8,128)(2,1)S(1)}, u32[]{:S(2)}, u32[]{:S(2)}) async-start(bf16[16,552,128]{2,1,0:T(8,128)(2,1)} %copy-done), calls=%async_computation.1 | async-start | bytes 4521984 | tf_op jit(solution)/shard_map/all_to_all | solution.py:63
  55.1 29.4 %collective-permute-start = (bf16[224,2048]{1,0:T(8,128)(2,1)S(1)}, bf16[224,2048]{1,0:T(8,128)(2,1)}, u32[]{:S(2)}, u32[]{:S(2)}) collective-permute-start(bf16[224,2048]{1,0:T(8,128)(2,1)S(1)} %bitcast.11), channel_id=1, source_target_pairs={{0,16},{16,0},{1,17},{17,1},{2,18},{18,2},{3,19},{19,3},{4,20},{20... | collective-permute-start | bytes 2752520 | tf_op jit(solution)/shard_map/ppermute | solution.py:221
  57.0 27.5 %collective-permute-start.1 = (bf16[224,2048]{1,0:T(8,128)(2,1)}, bf16[224,2048]{1,0:T(8,128)(2,1)}, u32[]{:S(2)}, u32[]{:S(2)}) collective-permute-start(bf16[224,2048]{1,0:T(8,128)(2,1)} %bitcast.13), channel_id=1, source_target_pairs={{0,16},{16,0},{1,17},{17,1},{2,18},{18,2},{3,19},{19,3},{4,20},{20... | collective-permute-start | bytes 2752520 | tf_op jit(solution)/shard_map/ppermute | solution.py:222
  82.4 2.1 %copy-start.2 = (bf16[1,2048,224]{1,2,0:T(8,128)(2,1)S(1)}, bf16[1,2048,224]{1,2,0:T(8,128)(2,1)}, u32[]{:S(2)}) copy-start(bf16[1,2048,224]{1,2,0:T(8,128)(2,1)} %param.13) | copy-start | bytes 2752516
  82.5 5.3 %collective-permute-start.2 = (bf16[16,224,128]{2,1,0:T(8,128)(2,1)S(1)}, bf16[16,224,128]{2,1,0:T(8,128)(2,1)S(1)}, u32[]{:S(2)}, u32[]{:S(2)}) collective-permute-start(bf16[16,224,128]{2,1,0:T(8,128)(2,1)S(1)} %slice.4), channel_id=1, source_target_pairs={{0,16},{16,0},{1,17},{17,1},{2,18},{18,2},{3,19},{19,3},{4,20},{20... | collective-permute-start | bytes 2752520 | tf_op jit(solution)/shard_map/ppermute | solution.py:238
  88.7 48.6 %copy-start.3 = (f32[128,2]{0,1:T(2,128)S(1)}, f32[128,2]{0,1:T(2,128)}, u32[]{:S(2)}) copy-start(f32[128,2]{0,1:T(2,128)} %param.11) | copy-start | bytes 3076
  88.7 66.9 %copy-start.4 = (f32[128]{0:T(128)S(1)}, f32[128]{0:T(128)}, u32[]{:S(2)}) copy-start(f32[128]{0:T(128)} %param.15) | copy-start | bytes 1540
  114.0 30.3 %all-to-all-start.3 = ((bf16[32,2,640]{2,1,0:T(2,128)(2,1)}), bf16[32,2,640]{2,1,0:T(2,128)(2,1)S(1)}, u32[]{:S(2)}, u32[]{:S(2)}) async-start(bf16[32,2,640]{2,1,0:T(2,128)(2,1)} %shard_map.86), calls=%async_computation.3 | async-start | bytes 163840 | tf_op jit(solution)/shard_map/all_to_all | solution.py:58

commit v8 on v7

--- a/solution.py
+++ b/solution.py
@@ -15,8 +15,10 @@
 W = D // TP
 HID = 224
 EXTRA = 8
-FIRST = 16
+FIRST = 20
+BACK = 18
 FIRST_TP = 10
+TURN = (BACK - FIRST) % EXPERTS
 FRONT = ROWS + EXTRA
 EPS = 1e-05
 
@@ -25,17 +27,18 @@
 MIB = 1 << 20
 
 
-def call(kernel, outs, mib, hbm=0, **kw):
+def call(kernel, outs, mib, hbm=0, far_out=False, **kw):
     def run(*operands):
         many = isinstance(outs, list)
         near = len(operands) - hbm
+        kept = [pltpu.HBM if far_out else pltpu.VMEM] + [pltpu.VMEM] * (len(outs) - 1)
         vmem = pl.BlockSpec(memory_space=pltpu.VMEM)
         spaces = [pltpu.VMEM] * near + [pltpu.HBM] * hbm
         return pl.pallas_call(
             kernel,
-            out_shape=[pltpu.VMEM(s, d) for s, d in outs] if many else pltpu.VMEM(*outs),
+            out_shape=[s(*out) for s, out in zip(kept, outs)] if many else pltpu.VMEM(*outs),
             in_specs=[pl.BlockSpec(memory_space=space) for space in spaces],
-            out_specs=[vmem] * len(outs) if many else vmem,
+            out_specs=[pl.BlockSpec(memory_space=s) for s in kept] if many else vmem,
             compiler_params=pltpu.CompilerParams(vmem_limit_bytes=mib * MIB),
             **kw,
         )(
@@ -53,8 +56,8 @@
     return (slot // 2) * (2 * EXPERTS) + 2 * position + slot % 2
 
 
-def exchange(blocks):
-    order = [(p + FIRST) % EXPERTS for p in range(EXPERTS)]
+def exchange(blocks, first):
+    order = [(p + first) % EXPERTS for p in range(EXPERTS)]
     return lax.all_to_all(blocks, "z", 0, 0, axis_index_groups=[order], tiled=True)
 
 
@@ -65,7 +68,7 @@
 
 def dispatch_kernel(
     routing_far, tokens_far, gain_far, out_ref, place_ref, gain_out_ref,
-    routing_ref, tokens_ref, gain_ref, sems,
+    routing_ref, tokens_ref, gain_ref, rows_ref, sems,
 ):
     copies = [
         pltpu.make_async_copy(routing_far, routing_ref, sems.at[0]),
@@ -89,15 +92,17 @@
     slot0 = jnp.sum(jnp.where(hit0, before, 0.0), axis=0, keepdims=True).astype(jnp.int32)
     slot1 = jnp.sum(jnp.where(hit1, before, 0.0), axis=0, keepdims=True).astype(jnp.int32)
     place0, place1 = place_of(slot0, expert0), place_of(slot1, expert1)
-    place_ref[0:1] = place0
-    place_ref[1:2] = place1
     spots = lax.broadcasted_iota(jnp.int32, (ROWS, TOK), 0)
     picker = jnp.where((spots == place0) | (spots == place1), 1.0, 0.0).astype(BF16)
     copies[1].wait()
     rows = jnp.dot(picker, tokens_ref[...], preferred_element_type=F32).astype(BF16)
     for block in range(CAP // 2):
         piece = rows[block * 64 : (block + 1) * 64]
-        out_ref[:, :, block * W : (block + 1) * W] = piece.reshape(EXPERTS, 2, W)
+        rows_ref[:, :, block * W : (block + 1) * W] = piece.reshape(EXPERTS, 2, W)
+    sent = pltpu.make_async_copy(rows_ref, out_ref, sems.at[3])
+    sent.start()
+    place_ref[0:1] = place0
+    place_ref[1:2] = place1
     copies[2].wait()
     gain = gain_ref[...]
     high = gain.astype(BF16).astype(F32)
@@ -106,6 +111,7 @@
     part = lax.broadcasted_iota(jnp.int32, (EXTRA, W), 0)
     parts = jnp.where(part == 0, high, jnp.where(part == 1, mid, jnp.where(part == 2, low, 0.0)))
     gain_out_ref[...] = parts.astype(BF16)
+    sent.wait()
 
 
 def prepare_kernel(place_ref, weight_ref, pick_ref, weight_out_ref):
@@ -171,13 +177,20 @@
         total = jnp.zeros((64, W), F32)
         for t in range(TP):
             total = total + parts_ref[t, block * 64 : (block + 1) * 64].astype(F32)
-        out_ref[:, :, block * W : (block + 1) * W] = total.astype(BF16).reshape(EXPERTS, 2, W)
+        piece = total.astype(BF16).reshape(EXPERTS, 2, W)
+        out_ref[: EXPERTS - TURN, :, block * W : (block + 1) * W] = piece[TURN:]
+        out_ref[EXPERTS - TURN :, :, block * W : (block + 1) * W] = piece[:TURN]
 
 
 def combine_kernel(rows_ref, pick_ref, weight_ref, mixed_ref, square_ref):
     rows = jnp.concatenate(
         [
-            rows_ref[:, :, block * W : (block + 1) * W].reshape(64, W)
+            jnp.concatenate(
+                [
+                    rows_ref[EXPERTS - TURN :, :, block * W : (block + 1) * W],
+                    rows_ref[: EXPERTS - TURN, :, block * W : (block + 1) * W],
+                ]
+            ).reshape(64, W)
             for block in range(CAP // 2)
         ],
         axis=0,
@@ -210,14 +223,16 @@
         [((EXPERTS, 2, 640), BF16), ((2, TOK), jnp.int32), ((EXTRA, W), BF16)],
         4,
         hbm=3,
+        far_out=True,
         scratch_shapes=[
             pltpu.VMEM((2, TOK), jnp.int32),
             pltpu.VMEM((TOK, W), BF16),
             pltpu.VMEM((1, W), F32),
-            pltpu.SemaphoreType.DMA((3,)),
+            pltpu.VMEM((EXPERTS, 2, 640), BF16),
+            pltpu.SemaphoreType.DMA((4,)),
         ],
     )(routing.T, tokens, norm_gain.reshape(1, W))
-    arrived = exchange(outgoing)
+    arrived = exchange(outgoing, FIRST)
     gate_other = lax.ppermute(gate_own, "c", swap)
     up_other = lax.ppermute(up_own, "c", swap)
     pick, weight = call(
@@ -247,7 +262,7 @@
     )
     parts = across_plane(parts)
     reduced = call(reduce_kernel, ((EXPERTS, 2, 640), BF16), 4)(parts)
-    returned = exchange(reduced)
+    returned = exchange(reduced, BACK)
     mixed, square = call(
         combine_kernel, [((TOK, W), F32), ((TP, 1, TOK), F32)], 4
     )(returned, pick, weight)

time: 157 us -> 158 us (level)
  starting transfers between devices: 37.5 us -> 35.8 us
  waiting for transfers between devices: 29.7 us -> 31.3 us
    all_to_all x1, starting transfers between devices: 23.3 us -> 21.6 us  [exchange(): lax.all_to_all(blocks, 'z', 0, 0, axis_index_groups=[order], tiled=True)]
    all_to_all x1, waiting for transfers between devices: 6.72 us -> 8.34 us  [exchange(): lax.all_to_all(blocks, 'z', 0, 0, axis_index_groups=[order], tiled=True)]
where the time goes in v8:
time: 158 us; the launch traced here: 157 us
  blocking collectives  79 us (50%)
  starting transfers between devices  35.8 us (23%)
  waiting for transfers between devices  31.3 us (20%)
  Pallas kernels  8.62 us (5%)
  local copies, waits for them, and re-layouts  2.08 us (1%)
    all_to_all x1, blocking collectives, exchange(): lax.all_to_all(blocks, 'z', 0, 0, axis_index_groups=[order], tiled=True)  43.6 us
    all_to_all x2, blocking collectives, across_plane(): lax.all_to_all(blocks, 't', 0, 0, axis_index_groups=[order], tiled=True)  35.4 us
    all_to_all x1, waiting for transfers between devices, across_plane(): lax.all_to_all(blocks, 't', 0, 0, axis_index_groups=[order], tiled=True)  22.9 us
    all_to_all x1, starting transfers between devices, exchange(): lax.all_to_all(blocks, 'z', 0, 0, axis_index_groups=[order], tiled=True)  21.6 us
    pallas_call x8, Pallas kernels, run(): pl.pallas_call(kernel, out_shape=[s(*out) for s, out in zip(kept, outs)]...  8.62 us
    all_to_all x1, waiting for transfers between devices, exchange(): lax.all_to_all(blocks, 'z', 0, 0, axis_index_groups=[order], tiled=True)  8.34 us
    all_to_all x1, starting transfers between devices, across_plane(): lax.all_to_all(blocks, 't', 0, 0, axis_index_groups=[order], tiled=True)  7.83 us
  transfers between devices with their start and end apart: 5, of which 2 were waited for; matrix products, arithmetic and copies ran while one was open for 0% of the time, Pallas kernels for 2%

profile of v8, /device:TPU:2, one launch (start us, length us, event | category | flops | bytes accessed | tf_op | source)
XLA Modules:
  0.0 156.9 jit_solution(12746657670953617744)
XLA Ops:
  0.0 1.7 %shard_map.82 = (bf16[32,2,640]{2,1,0:T(2,128)(2,1)}, s32[2,128]{1,0:T(2,128)S(1)}, bf16[8,128]{1,0:T(8,128)(2,1)S(1)}) custom-call(s32[2,128]{1,0:T(2,128)} %bitcast.18, bf16[128,128]{1,0:T(8,128)(2,1)} %tokens_far.1, f32[1,128]{1,0:T(1,128)} %bitcast.19), custom_call_target="tpu_custom_call" | custom-call | tf_op jit(solution)/shard_map/pallas_call | solution.py:37
  1.7 43.6 %all_to_all.25.rows_ref = bf16[32,2,640]{2,1,0:T(2,128)(2,1)S(1)} all-to-all(bf16[32,2,640]{2,1,0:T(2,128)(2,1)} %get-tuple-element.12), channel_id=1, replica_groups={{640,672,704,736,768,800,832,864,896,928,960,992,0,32,64,96,128,160,192..., dimensions={0} | all-to-all | bytes 163840 | tf_op jit(solution)/shard_map/all_to_all | solution.py:61
  45.3 1.3 shard_map.83
  46.6 0.0 copy-start
  46.6 1.4 copy-done
  48.0 0.0 copy-start.1
  48.0 7.8 %all-to-all-start.1 = ((bf16[16,552,128]{2,1,0:T(8,128)(2,1)}), bf16[16,552,128]{2,1,0:T(8,128)(2,1)S(1)}, u32[]{:S(2)}, u32[]{:S(2)}) async-start(bf16[16,552,128]{2,1,0:T(8,128)(2,1)} %copy-done), calls=%async_computation.1 | async-start | bytes 4521984 | tf_op jit(solution)/shard_map/all_to_all | solution.py:66
  55.9 0.0 copy-done.1
  55.9 1.9 %collective-permute-start = (bf16[224,2048]{1,0:T(8,128)(2,1)S(1)}, bf16[224,2048]{1,0:T(8,128)(2,1)}, u32[]{:S(2)}, u32[]{:S(2)}) collective-permute-start(bf16[224,2048]{1,0:T(8,128)(2,1)S(1)} %bitcast.11), channel_id=1, source_target_pairs={{0,16},{16,0},{1,17},{17,1},{2,18},{18,2},{3,19},{19,3},{4,20},{20... | collective-permute-start | bytes 2752520 | tf_op jit(solution)/shard_map/ppermute | solution.py:236
  57.8 2.4 %collective-permute-start.1 = (bf16[224,2048]{1,0:T(8,128)(2,1)}, bf16[224,2048]{1,0:T(8,128)(2,1)}, u32[]{:S(2)}, u32[]{:S(2)}) collective-permute-start(bf16[224,2048]{1,0:T(8,128)(2,1)} %bitcast.13), channel_id=1, source_target_pairs={{0,16},{16,0},{1,17},{17,1},{2,18},{18,2},{3,19},{19,3},{4,20},{20... | collective-permute-start | bytes 2752520 | tf_op jit(solution)/shard_map/ppermute | solution.py:237
  60.2 22.9 %all-to-all-done.1.x_ref = bf16[16,552,128]{2,1,0:T(8,128)(2,1)S(1)} async-done(((bf16[16,552,128]{2,1,0:T(8,128)(2,1)}), bf16[16,552,128]{2,1,0:T(8,128)(2,1)S(1)}, u32[]{:S(2)}, u32[]{:S(2)}) %all-to-all-start.1) | async-done | bytes 2261024 | tf_op jit(solution)/shard_map/all_to_all | solution.py:66
  83.1 0.1 slice.4
  83.2 2.1 %collective-permute-start.2 = (bf16[16,224,128]{2,1,0:T(8,128)(2,1)S(1)}, bf16[16,224,128]{2,1,0:T(8,128)(2,1)S(1)}, u32[]{:S(2)}, u32[]{:S(2)}) collective-permute-start(bf16[16,224,128]{2,1,0:T(8,128)(2,1)S(1)} %slice.4), channel_id=1, source_target_pairs={{0,16},{16,0},{1,17},{17,1},{2,18},{18,2},{3,19},{19,3},{4,20},{20... | collective-permute-start | bytes 2752520 | tf_op jit(solution)/shard_map/ppermute | solution.py:253
  85.3 0.0 collective-permute-done.gate_b
  85.3 0.0 collective-permute-done.1.up_b
  85.3 0.0 copy-done.2
  85.3 3.2 %shard_map.84.hidden_ref = bf16[2,320,224]{2,1,0:T(8,128)(2,1)S(1)} custom-call(bf16[16,552,128]{2,1,0:T(8,128)(2,1)S(1)} %all-to-all-done.1.x_ref, bf16[224,2048]{1,0:T(8,128)(2,1)S(1)} %bitcast.12, bf16[224,2048]{1,0:T(8,128)(2,1)} %collective-permute-done.gate_b, bf16[224,2048]{1,0:T(8,128)(2,1)S(1)} %bitcast.14, ...), custom_call_target="tpu_custom_call" | custom-call | tf_op jit(solution)/shard_map/pallas_call | solution.py:37
  88.6 0.0 collective-permute-done.2.down_ref
  88.6 0.8 shard_map.85
  89.4 0.0 copy-start.3
  89.4 0.0 copy-start.4
  89.4 24.4 %all_to_all.26.parts_ref = bf16[16,320,128]{2,1,0:T(8,128)(2,1)S(1)} all-to-all(bf16[16,320,128]{2,1,0:T(8,128)(2,1)S(1)} %shard_map.85), channel_id=1, replica_groups={{10,11,8,9,14,15,12,13,2,3,0,1,6,7,4,5},{26,27,24,25,30,31,28,29,18,19,..., dimensions={0} | all-to-all | bytes 2621440 | tf_op jit(solution)/shard_map/all_to_all | solution.py:66
  113.9 0.8 shard_map.86
  114.7 21.6 %all-to-all-start.3 = ((bf16[32,2,640]{2,1,0:T(2,128)(2,1)}), bf16[32,2,640]{2,1,0:T(2,128)(2,1)S(1)}, u32[]{:S(2)}, u32[]{:S(2)}) async-start(bf16[32,2,640]{2,1,0:T(2,128)(2,1)} %shard_map.86), calls=%async_computation.3 | async-start | bytes 163840 | tf_op jit(solution)/shard_map/all_to_all | solution.py:61
  136.3 0.0 copy-done.3
  136.3 0.2 shard_map.87
  136.6 8.3 %all-to-all-done.3.rows_ref = bf16[32,2,640]{2,1,0:T(2,128)(2,1)S(1)} async-done(((bf16[32,2,640]{2,1,0:T(2,128)(2,1)}), bf16[32,2,640]{2,1,0:T(2,128)(2,1)S(1)}, u32[]{:S(2)}, u32[]{:S(2)}) %all-to-all-start.3) | async-done | bytes 81952 | tf_op jit(solution)/shard_map/all_to_all | solution.py:61
  144.9 0.3 shard_map.88
  145.2 11.0 %all_to_all.27.square_ref = f32[16,1,128]{2,1,0:T(1,128)S(1)} all-to-all(f32[16,1,128]{2,1,0:T(1,128)S(1)} %get-tuple-element.18), channel_id=1, replica_groups={{10,11,8,9,14,15,12,13,2,3,0,1,6,7,4,5},{26,27,24,25,30,31,28,29,18,19,..., dimensions={0} | all-to-all | bytes 16384 | tf_op jit(solution)/shard_map/all_to_all | solution.py:66
  156.2 0.0 copy-done.4
  156.2 0.1 shard_map.89
  156.3 0.6 copy.9
  (1 shorter events, 0.0 us)
Async XLA Ops:
  46.6 1.4 copy-start
  48.0 7.8 %copy-start.1 = (bf16[1,2048,224]{1,2,0:T(8,128)(2,1)S(1)}, bf16[1,2048,224]{1,2,0:T(8,128)(2,1)}, u32[]{:S(2)}) copy-start(bf16[1,2048,224]{1,2,0:T(8,128)(2,1)} %param.12) | copy-start | bytes 2752516
  48.0 35.1 %all-to-all-start.1 = ((bf16[16,552,128]{2,1,0:T(8,128)(2,1)}), bf16[16,552,128]{2,1,0:T(8,128)(2,1)S(1)}, u32[]{:S(2)}, u32[]{:S(2)}) async-start(bf16[16,552,128]{2,1,0:T(8,128)(2,1)} %copy-done), calls=%async_computation.1 | async-start | bytes 4521984 | tf_op jit(solution)/shard_map/all_to_all | solution.py:66
  55.9 29.4 %collective-permute-start = (bf16[224,2048]{1,0:T(8,128)(2,1)S(1)}, bf16[224,2048]{1,0:T(8,128)(2,1)}, u32[]{:S(2)}, u32[]{:S(2)}) collective-permute-start(bf16[224,2048]{1,0:T(8,128)(2,1)S(1)} %bitcast.11), channel_id=1, source_target_pairs={{0,16},{16,0},{1,17},{17,1},{2,18},{18,2},{3,19},{19,3},{4,20},{20... | collective-permute-start | bytes 2752520 | tf_op jit(solution)/shard_map/ppermute | solution.py:236
  57.8 27.5 %collective-permute-start.1 = (bf16[224,2048]{1,0:T(8,128)(2,1)}, bf16[224,2048]{1,0:T(8,128)(2,1)}, u32[]{:S(2)}, u32[]{:S(2)}) collective-permute-start(bf16[224,2048]{1,0:T(8,128)(2,1)} %bitcast.13), channel_id=1, source_target_pairs={{0,16},{16,0},{1,17},{17,1},{2,18},{18,2},{3,19},{19,3},{4,20},{20... | collective-permute-start | bytes 2752520 | tf_op jit(solution)/shard_map/ppermute | solution.py:237
  83.1 2.1 %copy-start.2 = (bf16[1,2048,224]{1,2,0:T(8,128)(2,1)S(1)}, bf16[1,2048,224]{1,2,0:T(8,128)(2,1)}, u32[]{:S(2)}) copy-start(bf16[1,2048,224]{1,2,0:T(8,128)(2,1)} %param.13) | copy-start | bytes 2752516
  83.2 5.3 %collective-permute-start.2 = (bf16[16,224,128]{2,1,0:T(8,128)(2,1)S(1)}, bf16[16,224,128]{2,1,0:T(8,128)(2,1)S(1)}, u32[]{:S(2)}, u32[]{:S(2)}) collective-permute-start(bf16[16,224,128]{2,1,0:T(8,128)(2,1)S(1)} %slice.4), channel_id=1, source_target_pairs={{0,16},{16,0},{1,17},{17,1},{2,18},{18,2},{3,19},{19,3},{4,20},{20... | collective-permute-start | bytes 2752520 | tf_op jit(solution)/shard_map/ppermute | solution.py:253
  89.4 46.9 %copy-start.3 = (f32[128,2]{0,1:T(2,128)S(1)}, f32[128,2]{0,1:T(2,128)}, u32[]{:S(2)}) copy-start(f32[128,2]{0,1:T(2,128)} %param.11) | copy-start | bytes 3076
  89.4 66.8 %copy-start.4 = (f32[128]{0:T(128)S(1)}, f32[128]{0:T(128)}, u32[]{:S(2)}) copy-start(f32[128]{0:T(128)} %param.15) | copy-start | bytes 1540
  114.7 30.2 %all-to-all-start.3 = ((bf16[32,2,640]{2,1,0:T(2,128)(2,1)}), bf16[32,2,640]{2,1,0:T(2,128)(2,1)S(1)}, u32[]{:S(2)}, u32[]{:S(2)}) async-start(bf16[32,2,640]{2,1,0:T(2,128)(2,1)} %shard_map.86), calls=%async_computation.3 | async-start | bytes 163840 | tf_op jit(solution)/shard_map/all_to_all | solution.py:61
